TPU v7x, 32 devices: a whole 2x2x4 slice. The times are simulated.
32 devices in a mesh: sp: 8 (over z, x), tp: 4 (over y, core).
Axes of the slice: x: 2, y: 2, z: 4, core: 2. Of those that a mesh axis runs over, the one named last changes fastest.
Arguments:
- readout_query_vectors: bfloat16 [2048, 2048], P('sp', 'tp'), may hold values from -6 to 6
- attention_key_vectors: bfloat16 [2048, 2048], P('sp', 'tp'), may hold values from -6 to 6
- attention_content_vectors: bfloat16 [2048, 2048], P('sp', 'tp'), may hold values from -6 to 6
- step_size_preactivation: bfloat16 [2048, 2048], P('sp', 'tp'), may hold values from -16 to 8
- forgetting_preactivation: float32 [2048, 2048], P('sp', 'tp'), may hold values from -22 to 3
- extra_forgetting_bias: float32 [2048, 32], P('sp', 'tp'), may hold values from -0.7 to 0
- subspace_normalizer_gain: float32 [2048], P('tp'), may hold values from 0.1 to 1.9
- skip_connection_stream: bfloat16 [2048, 2048], P('sp'), may hold values from -40 to 40
- blender_projection_matrix: bfloat16 [2048, 2048], P('tp'), may hold values from -0.125 to 0.125
- specialist_prenormal_gain: float32 [2048], replicated, may hold values from 0.1 to 1.9
- cluster_router_chance: float32 [2048], P('sp'), may hold values from 0.4 to 1
- specialist_chance_within_cluster: float32 [2048, 2], P('sp'), may hold values from 0.1 to 1
- chosen_specialist_ids: int32 [2048, 2], P('sp'), may hold values from 0 to 7, all different within a row; in each aligned block of 256 rows (0 to 255, 256 to 511, ...) at most 128 rows name the same one
- specialist_switch_matrix: bfloat16 [8, 2048, 2048], P('sp', None, 'tp'), may hold values from -0.125 to 0.125
- specialist_expansion_matrix: bfloat16 [8, 2048, 2048], P('sp', None, 'tp'), may hold values from -0.125 to 0.125
- specialist_contraction_matrix: bfloat16 [8, 2048, 2048], P('sp', 'tp'), may hold values from -0.375 to 0.375
Outputs:
- layer_out: bfloat16 [2048, 2048], P('sp')
Inputs may be any that keep to these rules, and one draw needn't show every extreme that they name: `chosen_specialist_ids`: in each aligned block of 256 rows every expert is named at most 128 times.
All inputs are finite; a program needn't handle non-finite values.
Results may differ from a plain program's by a relative error of at most 0.022.
Values may be sent and summed in bfloat16 or wider, within the bound.
A program may use at most 64 MiB of HBM per device.

v0:
```python
import functools
import math

import jax
import jax.numpy as jnp
from jax import lax
from jax.experimental import pallas as pl
from jax.experimental.pallas import tpu as pltpu
from jax.sharding import PartitionSpec as P

MESH = pl.DeviceIdType.MESH
F32 = jnp.float32
BF16 = jnp.bfloat16


def dot(left, right, axes=(1, 0)):
    return lax.dot_general(
        left, right, (((axes[0],), (axes[1],)), ((), ())), preferred_element_type=F32
    )


def halves(data):
    high = data.astype(BF16)
    return high, (data - high.astype(F32)).astype(BF16)


def dot3(left, right, axes=(1, 0)):
    lh, ll = halves(left)
    rh, rl = halves(right)
    return dot(lh, rh, axes) + (dot(lh, rl, axes) + dot(ll, rh, axes))


def dot1(left, right, axes=(1, 0)):
    return dot(left.astype(BF16), right.astype(BF16), axes)


def mixer_kernel(head_dim, segment, q_ref, k_ref, v_ref, a_ref, f_ref, b_ref, out_ref, map_ref, ka_ref):
    pair = pl.program_id(0)
    rows, width = q_ref.shape
    blocks = rows // segment
    per = width // head_dim
    shift = segment.bit_length() - 1
    row = lax.broadcasted_iota(jnp.int32, (rows, rows), 0)
    col = lax.broadcasted_iota(jnp.int32, (rows, rows), 1)
    same = (row >> shift) == (col >> shift)
    strict = same & (row > col)
    inclusive = same & (row >= col)
    triangle = jnp.where(inclusive, 1.0, 0.0).astype(BF16)
    lane = lax.broadcasted_iota(jnp.int32, (rows, width), 1)
    bias = b_ref[...]
    bias_lane = lax.broadcasted_iota(jnp.int32, bias.shape, 1)

    def spread(values):
        total = values[per - 1]
        for h in range(per - 2, -1, -1):
            total = jnp.where(lane < (h + 1) * head_dim, values[h], total)
        return total

    own_bias = [
        jnp.sum(jnp.where(bias_lane == pair * per + h, bias, 0.0), axis=1, keepdims=True)
        for h in range(per)
    ]
    decay = -(0.6065306597126334 / (1.0 + jnp.exp(-f_ref[...]))) + spread(own_bias)
    high, low = halves(decay)
    lowest = (decay - high.astype(F32) - low.astype(F32)).astype(BF16)
    cumulative = dot(triangle, high) + (dot(triangle, low) + dot(triangle, lowest))
    closing_rows = cumulative.reshape(blocks, segment, width)[:, segment - 1 :, :]
    closing = jnp.broadcast_to(closing_rows, (blocks, segment, width)).reshape(rows, width)
    keys = k_ref[...].astype(F32)
    squares = keys * keys
    norms = spread(
        [
            jnp.sum(squares[:, h * head_dim : (h + 1) * head_dim], axis=1, keepdims=True)
            for h in range(per)
        ]
    )
    removal = keys * lax.rsqrt(norms + 1e-06)
    rate = 1.0 / (1.0 + jnp.exp(-a_ref[...].astype(F32)))
    beta = removal * rate
    grow = jnp.exp(-cumulative)
    fade = jnp.exp(closing - cumulative)
    alpha_all = -removal * jnp.exp(cumulative - decay)
    beta_hat_all = beta * grow
    key_hat_all = keys * grow
    query_all = q_ref[...].astype(F32) * jnp.exp(cumulative)
    beta_bar_all = beta * fade
    key_bar_all = keys * fade
    values_all = v_ref[...]
    keep_all = jnp.exp(closing_rows)
    eye = lax.broadcasted_iota(jnp.int32, (head_dim, head_dim), 0) == lax.broadcasted_iota(
        jnp.int32, (head_dim, head_dim), 1
    )
    outs, maps = [], []
    for h in range(per):
        part = slice(h * head_dim, (h + 1) * head_dim)
        alpha, beta_hat, key_hat = alpha_all[:, part], beta_hat_all[:, part], key_hat_all[:, part]
        query, values = query_all[:, part], values_all[:, part]
        beta_bar, key_bar = beta_bar_all[:, part], key_bar_all[:, part]
        lower = jnp.where(strict, dot3(alpha, beta_hat, (1, 1)), 0.0)
        remove_write = jnp.where(strict, dot1(alpha, key_hat, (1, 1)), 0.0)
        read_remove = jnp.where(inclusive, dot1(query, beta_hat, (1, 1)), 0.0)
        read_write = jnp.where(inclusive, dot1(query, key_hat, (1, 1)), 0.0)
        lh, ll = halves(lower)
        inverse = jnp.where(row == col, 1.0, jnp.where((row >> 1) == (col >> 1), lower, 0.0))
        for s in range(1, shift):
            off = ((row >> (s + 1)) == (col >> (s + 1))) & ((row >> s) != (col >> s))
            near = inverse.astype(BF16)
            reach = dot(jnp.where(off, lower, 0.0).astype(BF16), near)
            inverse = inverse + dot(near, reach.astype(BF16))
        wh, wl = halves(remove_write)
        side = jnp.concatenate([alpha, dot(wh, values) + dot(wl, values)], axis=1)
        near = inverse.astype(BF16)
        solved = dot(near, side.astype(BF16))
        sh, sl = halves(solved)
        miss = side - solved + (dot(lh, sh) + (dot(lh, sl) + dot(ll, sh)))
        solved = solved + dot(near, miss.astype(BF16))
        read = dot1(read_remove, solved)
        read_map = query + read[:, :head_dim]
        local = read[:, head_dim:] + dot(read_write.astype(BF16), values)
        state = jnp.concatenate(
            [jnp.where(eye, 1.0, 0.0), jnp.zeros((head_dim, head_dim), F32)], axis=0
        )
        out_rows, map_rows = [], []
        for b in range(blocks):
            at = slice(b * segment, (b + 1) * segment)
            seen = dot1(read_map[at], state, (1, 1))
            map_rows.append(seen[:, :head_dim])
            out_rows.append(local[at] + seen[:, head_dim:])
            step = dot3(solved[at], beta_bar[at], (0, 0))
            bh, bl = halves(key_bar[at])
            add = step[head_dim:] + dot(values[at], bh, (0, 0)) + dot(values[at], bl, (0, 0))
            keep = step[:head_dim] + jnp.where(eye, keep_all[b][:, part], 0.0)
            state = dot3(state, keep)
            state = jnp.concatenate([state[:head_dim], state[head_dim:] + add], axis=0)
        outs.append(jnp.concatenate(out_rows, axis=0))
        maps.append(jnp.concatenate(map_rows, axis=0))
        ka_ref[h] = jnp.concatenate([state[:head_dim], state[head_dim:]], axis=1).astype(BF16)
    out_ref[...] = jnp.concatenate(outs, axis=1)
    map_ref[...] = jnp.concatenate(maps, axis=1).astype(BF16)


def exchange_kernel(count, per, workers, ka_ref, st_ref, got, fold, send1, recv1, send2, recv2):
    me = lax.axis_index("sp")
    dim = ka_ref.shape[1]
    barrier = pltpu.get_barrier_semaphore()
    for d in range(1, count):
        pl.semaphore_signal(
            barrier, inc=1, device_id={"sp": lax.rem(me + d, count)}, device_id_type=MESH
        )
    pl.semaphore_wait(barrier, count - 1)

    def first(t, owner):
        return pltpu.make_async_remote_copy(
            src_ref=ka_ref.at[pl.ds(t * per, per)],
            dst_ref=got.at[owner],
            send_sem=send1.at[t],
            recv_sem=recv1.at[owner],
            device_id={"sp": t},
            device_id_type=MESH,
        )

    def second(t, owner):
        return pltpu.make_async_remote_copy(
            src_ref=fold.at[t],
            dst_ref=st_ref.at[pl.ds(owner * per, per)],
            send_sem=send2.at[t],
            recv_sem=recv2.at[owner],
            device_id={"sp": t},
            device_id_type=MESH,
        )

    for t in range(workers):
        @pl.when(t != me)
        def _(t=t):
            first(t, me).start()

    def work():
        got[me] = ka_ref[pl.ds(me * per, per)]
        state = [jnp.zeros((dim, dim), F32) for _ in range(per)]
        for j in range(count):
            @pl.when(j != me)
            def _(j=j):
                pltpu.make_async_remote_copy(
                    src_ref=got.at[j],
                    dst_ref=got.at[j],
                    send_sem=send1.at[0],
                    recv_sem=recv1.at[j],
                    device_id={"sp": j},
                    device_id_type=MESH,
                ).wait_recv()
            for i in range(per):
                fold[j, i] = jnp.concatenate([state[i], jnp.zeros_like(state[i])], axis=1).astype(BF16)
                both = got[j, i]
                keep, add = both[:, :dim], both[:, dim:].astype(F32)
                sh, sl = halves(state[i])
                state[i] = dot(sh, keep) + dot(sl, keep) + add
        for t in range(count):
            @pl.when(t != me)
            def _(t=t):
                second(t, me).start()
        st_ref[pl.ds(me * per, per)] = fold[me]
        for t in range(count):
            @pl.when(t != me)
            def _(t=t):
                second(t, me).wait_send()

    if workers == count:
        work()
    else:
        pl.when(me < workers)(work)
    for t in range(workers):
        @pl.when(t != me)
        def _(t=t):
            first(t, me).wait_send()
            pltpu.make_async_remote_copy(
                src_ref=fold.at[t],
                dst_ref=st_ref.at[pl.ds(t * per, per)],
                send_sem=send2.at[0],
                recv_sem=recv2.at[t],
                device_id={"sp": t},
                device_id_type=MESH,
            ).wait_recv()


def finish_kernel(head_dim, out_ref, map_ref, st_ref, gain_ref, w_ref, part_ref, mixed):
    @pl.when(pl.program_id(0) == 0)
    def _():
        for h in range(out_ref.shape[1] // head_dim):
            part = slice(h * head_dim, (h + 1) * head_dim)
            states = st_ref[h][:, :head_dim]
            output = out_ref[:, part] + dot(map_ref[:, part], states, (1, 1))
            centered = output - jnp.mean(output, axis=1, keepdims=True)
            spread = jnp.mean(centered * centered, axis=1, keepdims=True)
            mixed[:, part] = (centered * lax.rsqrt(spread + 0.00064) * gain_ref[:, part]).astype(BF16)

    part_ref[...] = dot(mixed[...], w_ref[...]).astype(BF16)


def mixer_branch(query, key, value, step, forget, bias, gain, blender):
    count = lax.axis_size("sp")
    rows, channels = query.shape
    heads = bias.shape[1]
    head_dim = channels // heads
    segment = min(64, rows)
    width = 2 * head_dim
    pairs = heads // 2
    block = pl.BlockSpec((rows, width), lambda p: (0, p))
    out, maps, ka = pl.pallas_call(
        functools.partial(mixer_kernel, head_dim, segment),
        grid=(pairs,),
        in_specs=[block] * 5 + [pl.BlockSpec((rows, heads), lambda p: (0, 0))],
        out_specs=[block, block, pl.BlockSpec((2, head_dim, width), lambda p: (p, 0, 0))],
        out_shape=[
            jax.ShapeDtypeStruct((rows, channels), F32),
            jax.ShapeDtypeStruct((rows, channels), BF16),
            jax.ShapeDtypeStruct((heads, head_dim, width), BF16),
        ],
        compiler_params=pltpu.CompilerParams(vmem_limit_bytes=61 * 1024 * 1024),
    )(query, key, value, step, forget, bias)
    per = max(1, heads // count)
    workers = heads // per
    vmem = pl.BlockSpec(memory_space=pltpu.VMEM)
    states = pl.pallas_call(
        functools.partial(exchange_kernel, count, per, workers),
        out_shape=jax.ShapeDtypeStruct((heads, head_dim, width), BF16),
        in_specs=[vmem],
        out_specs=vmem,
        scratch_shapes=[
            pltpu.VMEM((count, per, head_dim, width), BF16),
            pltpu.VMEM((count, per, head_dim, width), BF16),
            pltpu.SemaphoreType.DMA((count,)),
            pltpu.SemaphoreType.DMA((count,)),
            pltpu.SemaphoreType.DMA((count,)),
            pltpu.SemaphoreType.DMA((count,)),
        ],
        compiler_params=pltpu.CompilerParams(collective_id=1, has_side_effects=True),
    )(ka)
    model_width = blender.shape[1]
    tile = min(512, model_width)
    whole = lambda *shape: pl.BlockSpec(shape, lambda p: (0,) * len(shape))
    return pl.pallas_call(
        functools.partial(finish_kernel, head_dim),
        grid=(model_width // tile,),
        in_specs=[
            whole(rows, channels),
            whole(rows, channels),
            whole(heads, head_dim, width),
            whole(1, channels),
            pl.BlockSpec((channels, tile), lambda p: (0, p)),
        ],
        out_specs=pl.BlockSpec((rows, tile), lambda p: (0, p)),
        out_shape=jax.ShapeDtypeStruct((rows, model_width), BF16),
        scratch_shapes=[pltpu.VMEM((rows, channels), BF16)],
    )(out, maps, states, gain.reshape(1, channels), blender)


def greet(sp_count, tp_count, sp, tp):
    barrier = pltpu.get_barrier_semaphore()
    for d in range(1, sp_count):
        pl.semaphore_signal(
            barrier, inc=1, device_id={"sp": lax.rem(sp + d, sp_count)}, device_id_type=MESH
        )
    for d in range(1, tp_count):
        pl.semaphore_signal(
            barrier, inc=1, device_id={"tp": lax.rem(tp + d, tp_count)}, device_id_type=MESH
        )
    pl.semaphore_wait(barrier, sp_count + tp_count - 2)


def copy_to(src, dst, send, recv, device):
    return pltpu.make_async_remote_copy(
        src_ref=src,
        dst_ref=dst,
        send_sem=send,
        recv_sem=recv,
        device_id=device,
        device_id_type=MESH,
    )


def span(index, size):
    return pl.ds(pl.multiple_of(index * size, size), size)


def row_total(data, terms):
    ones = jnp.ones((8, data.shape[1]), BF16)
    total = None
    for _ in range(terms):
        piece = data.astype(BF16)
        data = data - piece.astype(F32)
        product = dot(ones, piece, (1, 1))
        total = product if total is None else total + product
    return total


def route_kernel(
    sp_count, tp_count, experts, capacity,
    part_ref, skip_ref, gain_ref, ids_ref,
    hidden_ref, slot_ref, rows_ref,
    gathered, squares, outgoing,
    s_part, r_part, s_sq, r_sq, s_out, r_out, s_own, s_fwd, r_col,
):
    sp, tp = lax.axis_index("sp"), lax.axis_index("tp")
    rows, model = part_ref.shape
    cols = model // tp_count
    mine = span(tp, cols)
    groups = tp_count // 2
    core, group = lax.rem(tp, 2), tp // 2
    sibling = group * 2 + 1 - core
    greet(sp_count, tp_count, sp, tp)

    def part_copy(p):
        return copy_to(
            part_ref.at[:, span(p, cols)], gathered.at[tp], s_part.at[p], r_part.at[tp], {"tp": p}
        )

    for d in range(1, tp_count):
        part_copy(lax.rem(tp + d, tp_count)).start()

    ids = ids_ref[...]
    top = ids.shape[1]
    lanes = lax.broadcasted_iota(jnp.int32, (rows, experts), 1)
    named = [ids[:, k : k + 1] == lanes for k in range(top)]
    anyone = sum(jnp.where(n, 1.0, 0.0) for n in named).astype(BF16)
    r0 = lax.broadcasted_iota(jnp.int32, (rows, rows), 0)
    r1 = lax.broadcasted_iota(jnp.int32, (rows, rows), 1)
    before = dot(jnp.where(r0 > r1, 1.0, 0.0).astype(BF16), anyone)
    slots = [
        jnp.sum(
            jnp.where(n, before + lanes.astype(F32) * capacity, 0.0), axis=1, keepdims=True
        ).astype(jnp.int32)
        for n in named
    ]
    slot_ref[...] = jnp.concatenate(slots, axis=1)

    branch = part_ref[:, mine].astype(F32)
    for d in range(1, tp_count):
        p = lax.rem(tp + d, tp_count)
        copy_to(gathered.at[p], gathered.at[p], s_part.at[p], r_part.at[p], {"tp": p}).wait_recv()
        branch = branch + gathered[p].astype(F32)
    hidden = skip_ref[:, mine].astype(F32) + branch
    hidden_ref[...] = hidden
    squares[tp] = row_total(hidden * hidden, 3)

    def square_copy(p):
        return copy_to(squares.at[tp], squares.at[tp], s_sq.at[p], r_sq.at[tp], {"tp": p})

    for d in range(1, tp_count):
        square_copy(lax.rem(tp + d, tp_count)).start()
    total = squares[tp]
    for d in range(1, tp_count):
        p = lax.rem(tp + d, tp_count)
        copy_to(squares.at[p], squares.at[p], s_sq.at[p], r_sq.at[p], {"tp": p}).wait_recv()
        total = total + squares[p]
    inverse = lax.rsqrt(total / model + 1e-06)
    first = jnp.where(lax.broadcasted_iota(jnp.int32, (8, 128), 0) == 0, 1.0, 0.0).astype(BF16)
    column = None
    for _ in range(3):
        piece = inverse.astype(BF16)
        inverse = inverse - piece.astype(F32)
        product = dot(piece, first, (0, 0))
        column = product if column is None else column + product
    normed = (hidden * column[:, :1] * gain_ref[:, mine]).astype(BF16)

    per = experts // sp_count * capacity
    places = lax.broadcasted_iota(jnp.int32, (rows, per), 1)

    def block_for(t):
        at = places + t * per
        chosen = (slots[0] == at)
        for s in slots[1:]:
            chosen = chosen | (s == at)
        return dot(jnp.where(chosen, 1.0, 0.0).astype(BF16), normed, (0, 0)).astype(BF16)

    def out_copy(t):
        return copy_to(
            outgoing.at[t], rows_ref.at[sp, :, mine], s_out.at[t], r_out.at[sp], {"sp": t}
        )

    def give(d, carry):
        t = lax.rem(sp + d, sp_count)
        outgoing[t] = block_for(t)
        out_copy(t).start()
        return carry

    lax.fori_loop(1, sp_count, give, 0)
    rows_ref[sp, :, mine] = block_for(sp)

    def own_copy(p, s):
        here = rows_ref.at[s, :, mine]
        return copy_to(here, here, s_own.at[p, s], r_col.at[tp, s], {"tp": p})

    def forward(o, s):
        here = rows_ref.at[s, :, span(o, cols)]
        return copy_to(here, here, s_fwd.at[o, s], r_col.at[o, s], {"tp": sibling})

    def arrived(o, s):
        here = rows_ref.at[s, :, span(o, cols)]
        copy_to(here, here, s_fwd.at[o, s], r_col.at[o, s], {"tp": sibling}).wait_recv()

    def peers():
        return [lax.rem(group + g, groups) * 2 + core for g in range(1, groups)]

    lag = 2

    def relay(d, carry):
        @pl.when(d < sp_count)
        def _():
            s = lax.rem(sp - d + sp_count, sp_count)

            @pl.when(d > 0)
            def _():
                here = rows_ref.at[s, :, mine]
                copy_to(here, here, s_out.at[s], r_out.at[s], {"sp": s}).wait_recv()

            for p in peers():
                own_copy(p, s).start()
            own_copy(sibling, s).start()

        @pl.when(d >= lag)
        def _():
            s = lax.rem(sp - (d - lag) + sp_count, sp_count)
            for o in peers():
                arrived(o, s)
                forward(o, s).start()

        return carry

    lax.fori_loop(0, sp_count + lag, relay, 0)

    def settle(s, carry):
        arrived(sibling, s)
        for g in range(1, groups):
            arrived(lax.rem(group + g, groups) * 2 + 1 - core, s)
        own_copy(sibling, s).wait_send()
        for p in peers():
            own_copy(p, s).wait_send()
            forward(p, s).wait_send()
        return carry

    lax.fori_loop(0, sp_count, settle, 0)

    def sent(d, carry):
        out_copy(lax.rem(sp + d, sp_count)).wait_send()
        return carry

    lax.fori_loop(1, sp_count, sent, 0)
    for d in range(1, tp_count):
        p = lax.rem(tp + d, tp_count)
        part_copy(p).wait_send()
        square_copy(p).wait_send()


def return_kernel(
    sp_count, tp_count,
    rows_ref, switch_ref, expand_ref, contract_ref, hidden_ref, slot_ref, weight_ref,
    out_ref,
    y_ref, from_sib, pair, from_peer, summed, back,
    s_sib, r_sib, s_peer, r_peer, s_back, r_back, s_own, s_fwd, r_col,
):
    sp, tp = lax.axis_index("sp"), lax.axis_index("tp")
    per, model = y_ref.shape[1:]
    rows = hidden_ref.shape[0]
    cols = model // tp_count
    mine = span(tp, cols)
    groups = tp_count // 2
    core, group = lax.rem(tp, 2), tp // 2
    sibling = group * 2 + 1 - core
    greet(sp_count, tp_count, sp, tp)

    def sib_copy(s, g):
        return copy_to(
            y_ref.at[s, :, span(g * 2 + 1 - core, cols)],
            from_sib.at[s, g],
            s_sib.at[s, g],
            r_sib.at[s, g],
            {"tp": sibling},
        )

    def peer_copy(s, g):
        return copy_to(
            pair.at[s, g],
            from_peer.at[s, group],
            s_peer.at[s, g],
            r_peer.at[s, group],
            {"tp": g * 2 + core},
        )

    def back_copy(t):
        return copy_to(summed.at[t], back.at[sp], s_back.at[t], r_back.at[sp], {"sp": t})

    def others():
        return [lax.rem(group + d, groups) for d in range(1, groups)]

    def order(d):
        return lax.rem(sp + 1 + d, sp_count)

    local = switch_ref.shape[0]
    capacity = per // local
    chunk = math.gcd(sp_count, max(1, 256 // capacity))
    chunks = sp_count // chunk

    def expert(i):
        at = [order(i * chunk + c) for c in range(chunk)]
        for e in range(local):
            inside = slice(e * capacity, (e + 1) * capacity)
            data = jnp.concatenate([rows_ref[s, inside, :] for s in at], axis=0)
            gate = dot(data, switch_ref[e])
            units = (gate / (1.0 + jnp.exp(-gate)) * dot(data, expand_ref[e])).astype(BF16)
            value = dot(units, contract_ref[e]).astype(BF16)
            for c in range(chunk):
                y_ref[at[c], inside, :] = value[c * capacity : (c + 1) * capacity]
        for s in at:
            for g in others():
                sib_copy(s, g).start()
            sib_copy(s, group).start()

    def meet(s):
        for g in others():
            sib_copy(s, g).wait_recv()
            pair[s, g] = (
                y_ref[s, :, span(g * 2 + core, cols)].astype(F32) + from_sib[s, g].astype(F32)
            ).astype(BF16)
            peer_copy(s, g).start()
        sib_copy(s, group).wait_recv()

    def total_up(s):
        total = y_ref[s, :, mine].astype(F32) + from_sib[s, group].astype(F32)
        for g in others():
            copy_to(
                from_peer.at[s, g],
                from_peer.at[s, g],
                s_peer.at[s, g],
                r_peer.at[s, g],
                {"tp": g * 2 + core},
            ).wait_recv()
            total = total + from_peer[s, g].astype(F32)

        @pl.when(s != sp)
        def _():
            summed[s] = total.astype(BF16)
            back_copy(s).start()

        @pl.when(s == sp)
        def _():
            back[s] = total.astype(BF16)

    def step(i, carry):
        @pl.when(i < chunks)
        def _():
            expert(i)

        @pl.when((i >= 1) & (i <= chunks))
        def _():
            for c in range(chunk):
                meet(order((i - 1) * chunk + c))

        @pl.when(i >= 2)
        def _():
            for c in range(chunk):
                total_up(order((i - 2) * chunk + c))

        return carry

    lax.fori_loop(0, chunks + 2, step, 0)
    slots = slot_ref[...]
    weights = weight_ref[...]
    places = lax.broadcasted_iota(jnp.int32, (rows, sp_count * per), 1)
    top = slots.shape[1]
    chosen = [jnp.where(slots[:, k : k + 1] == places, 1.0, 0.0).astype(BF16) for k in range(top)]

    def landed(d, carry):
        s = lax.rem(sp + d, sp_count)
        copy_to(back.at[s], back.at[s], s_back.at[s], r_back.at[s], {"sp": s}).wait_recv()
        return carry

    lax.fori_loop(1, sp_count, landed, 0)
    returned = back[...].reshape(sp_count * per, cols)
    result = hidden_ref[...] + sum(
        weights[:, k : k + 1] * dot(chosen[k], returned) for k in range(top)
    )
    out_ref[:, mine] = result.astype(BF16)

    def own_copy(p):
        here = out_ref.at[:, mine]
        return copy_to(here, here, s_own.at[p], r_col.at[tp], {"tp": p})

    def forward(o):
        here = out_ref.at[:, span(o, cols)]
        return copy_to(here, here, s_fwd.at[o], r_col.at[o], {"tp": sibling})

    peers = [g * 2 + core for g in others()]
    for p in peers:
        own_copy(p).start()
    own_copy(sibling).start()
    for p in peers:
        forward(p).wait_recv()
        forward(p).start()
    forward(sibling).wait_recv()
    for g in others():
        forward(g * 2 + 1 - core).wait_recv()
    own_copy(sibling).wait_send()
    for p in peers:
        own_copy(p).wait_send()
        forward(p).wait_send()

    def close(s, carry):
        sib_copy(s, group).wait_send()
        for g in others():
            sib_copy(s, g).wait_send()
            peer_copy(s, g).wait_send()
        return carry

    lax.fori_loop(0, sp_count, close, 0)

    def sent(d, carry):
        back_copy(lax.rem(sp + d, sp_count)).wait_send()
        return carry

    lax.fori_loop(1, sp_count, sent, 0)


def body(
    readout_query_vectors,
    attention_key_vectors,
    attention_content_vectors,
    step_size_preactivation,
    forgetting_preactivation,
    extra_forgetting_bias,
    subspace_normalizer_gain,
    skip_connection_stream,
    blender_projection_matrix,
    specialist_prenormal_gain,
    cluster_router_chance,
    specialist_chance_within_cluster,
    chosen_specialist_ids,
    specialist_switch_matrix,
    specialist_expansion_matrix,
    specialist_contraction_matrix,
):
    partial_branch = mixer_branch(
        readout_query_vectors,
        attention_key_vectors,
        attention_content_vectors,
        step_size_preactivation,
        forgetting_preactivation,
        extra_forgetting_bias,
        subspace_normalizer_gain,
        blender_projection_matrix,
    )
    tok_rows, model_width = skip_connection_stream.shape
    sp_count, tp_count = lax.axis_size("sp"), lax.axis_size("tp")
    local_experts = specialist_switch_matrix.shape[0]
    experts = local_experts * sp_count
    top_count = chosen_specialist_ids.shape[1]
    capacity = 2 * tok_rows * top_count // experts
    cols = model_width // tp_count
    per = local_experts * capacity
    groups = tp_count // 2
    vmem = pl.BlockSpec(memory_space=pltpu.VMEM)
    sems = pltpu.SemaphoreType.DMA
    hidden_cols, slots, rows_in = pl.pallas_call(
        functools.partial(route_kernel, sp_count, tp_count, experts, capacity),
        out_shape=[
            jax.ShapeDtypeStruct((tok_rows, cols), F32),
            jax.ShapeDtypeStruct((tok_rows, top_count), jnp.int32),
            jax.ShapeDtypeStruct((sp_count, per, model_width), BF16),
        ],
        in_specs=[vmem] * 4,
        out_specs=[vmem] * 3,
        scratch_shapes=[
            pltpu.VMEM((tp_count, tok_rows, cols), BF16),
            pltpu.VMEM((tp_count, 8, tok_rows), F32),
            pltpu.VMEM((sp_count, per, cols), BF16),
            sems((tp_count,)),
            sems((tp_count,)),
            sems((tp_count,)),
            sems((tp_count,)),
            sems((sp_count,)),
            sems((sp_count,)),
            sems((tp_count, sp_count)),
            sems((tp_count, sp_count)),
            sems((tp_count, sp_count)),
        ],
        compiler_params=pltpu.CompilerParams(
            collective_id=2, has_side_effects=True, vmem_limit_bytes=40 * 1024 * 1024
        ),
    )(
        partial_branch,
        skip_connection_stream,
        specialist_prenormal_gain.reshape(1, model_width),
        chosen_specialist_ids,
    )
    route_weight = (
        cluster_router_chance[:, None]
        * specialist_chance_within_cluster
        / jnp.sum(specialist_chance_within_cluster, axis=1, keepdims=True)
    )
    return pl.pallas_call(
        functools.partial(return_kernel, sp_count, tp_count),
        out_shape=jax.ShapeDtypeStruct((tok_rows, model_width), BF16),
        in_specs=[vmem] * 7,
        out_specs=vmem,
        scratch_shapes=[
            pltpu.VMEM((sp_count, per, model_width), BF16),
            pltpu.VMEM((sp_count, groups, per, cols), BF16),
            pltpu.VMEM((sp_count, groups, per, cols), BF16),
            pltpu.VMEM((sp_count, groups, per, cols), BF16),
            pltpu.VMEM((sp_count, per, cols), BF16),
            pltpu.VMEM((sp_count, per, cols), BF16),
            sems((sp_count, groups)),
            sems((sp_count, groups)),
            sems((sp_count, groups)),
            sems((sp_count, groups)),
            sems((sp_count,)),
            sems((sp_count,)),
            sems((tp_count,)),
            sems((tp_count,)),
            sems((tp_count,)),
        ],
        compiler_params=pltpu.CompilerParams(
            collective_id=3, has_side_effects=True, vmem_limit_bytes=50 * 1024 * 1024
        ),
    )(
        rows_in,
        specialist_switch_matrix,
        specialist_expansion_matrix,
        specialist_contraction_matrix,
        hidden_cols,
        slots,
        route_weight,
    )


def solution(mesh):
    in_specs = (
        P("sp", "tp"),
        P("sp", "tp"),
        P("sp", "tp"),
        P("sp", "tp"),
        P("sp", "tp"),
        P("sp", "tp"),
        P("tp"),
        P("sp", None),
        P("tp", None),
        P(),
        P("sp"),
        P("sp", None),
        P("sp", None),
        P("sp", None, "tp"),
        P("sp", None, "tp"),
        P("sp", "tp", None),
    )
    out_specs = P("sp", None)
    return jax.shard_map(body, mesh=mesh, in_specs=in_specs, out_specs=out_specs, check_vma=False)
```

profile of v0, /device:TPU:0, one launch (start us, length us, event | category | flops | bytes accessed | tf_op | source)
XLA Modules:
  0.0 175.9 jit_solution(18038447970227625506)
XLA Ops:
  0.0 1.5 copy.21.b_ref
  1.5 39.0 %shard_map.154 = (f32[256,512]{1,0:T(8,128)}, bf16[256,512]{1,0:T(8,128)(2,1)}, bf16[8,64,128]{2,1,0:T(8,128)(2,1)}) custom-call(bf16[256,512]{1,0:T(8,128)(2,1)} %q_ref.1, bf16[256,512]{1,0:T(8,128)(2,1)} %k_ref.1, bf16[256,512]{1,0:T(8,128)(2,1)} %v_ref.1, bf16[256,512]{1,0:T(8,128)(2,1)} %a_ref.1, f32[256,512]{1,0:T(8,128)} %f_ref.1, f32[256,8]{1,0:T(8,128)} %copy.21.b_ref), custom_call_target="tpu_custom_call" | custom-call | tf_op jit(solution)/shard_map/pallas_call | solution.py:248
  40.5 17.8 %shard_map.155.st_ref = bf16[8,64,128]{2,1,0:T(8,128)(2,1)} custom-call(bf16[8,64,128]{2,1,0:T(8,128)(2,1)} %get-tuple-element.13.ka_ref), custom_call_target="tpu_custom_call" | custom-call | tf_op jit(solution)/shard_map/pallas_call | solution.py:263
  58.3 0.0 copy-start.7
  58.3 0.0 copy-start.3
  58.3 0.0 copy-start.6
  58.3 0.0 copy-start.2
  58.4 7.0 %shard_map.156.part_ref = bf16[256,2048]{1,0:T(8,128)(2,1)} custom-call(f32[256,512]{1,0:T(8,128)} %get-tuple-element.11.out_ref, bf16[256,512]{1,0:T(8,128)(2,1)} %get-tuple-element.12.map_ref, bf16[8,64,128]{2,1,0:T(8,128)(2,1)} %shard_map.155.st_ref, f32[1,512]{1,0:T(1,128)} %bitcast.3, bf16[512,2048]{1,0:T(8,128)(2,1)} %w_ref.1), custom_call_target="tpu_custom_call" | custom-call | tf_op jit(solution)/shard_map/pallas_call | solution.py:281
  65.4 0.0 copy-done.7
  65.4 0.0 copy-start.8
  65.4 0.0 copy-start.9
  65.4 0.1 copy.22.ids_ref
  65.5 0.0 copy-done.3
  65.5 0.0 copy-done.6
  65.5 0.0 copy-start.1
  65.5 1.2 copy-done.1
  66.8 52.2 %shard_map.157 = (f32[256,512]{1,0:T(8,128)S(1)}, s32[256,2]{1,0:T(8,128)S(1)}, bf16[8,128,2048]{2,1,0:T(8,128)(2,1)S(1)}) custom-call(bf16[256,2048]{1,0:T(8,128)(2,1)S(1)} %copy-done.1, bf16[256,2048]{1,0:T(8,128)(2,1)S(1)} %copy-done.3, f32[1,2048]{1,0:T(1,128)S(1)} %bitcast.2, s32[256,2]{1,0:T(8,128)S(1)} %copy.22.ids_ref), custom_call_target="tpu_custom_call" | custom-call | tf_op jit(solution)/shard_map/pallas_call | solution.py:702
  119.0 0.0 copy-start
  119.0 1.9 %copy-done = bf16[8,128,2048]{2,1,0:T(8,128)(2,1)} copy-done((bf16[8,128,2048]{2,1,0:T(8,128)(2,1)}, bf16[8,128,2048]{2,1,0:T(8,128)(2,1)S(1)}, u32[]{:S(2)}) %copy-start) | copy-done | bytes 4194328
  121.0 0.0 copy-start.4
  121.0 0.8 copy-done.4
  121.8 0.0 copy-done.8
  121.8 0.0 copy-done.9
  121.8 0.1 copy.23
  121.9 0.1 broadcast_divide_fusion.weight_ref
  122.0 0.0 copy-done.2
  122.0 0.0 copy-start.5
  122.1 1.0 copy-done.5
  123.1 51.9 %shard_map.158 = bf16[256,2048]{1,0:T(8,128)(2,1)S(1)} custom-call(bf16[8,128,2048]{2,1,0:T(8,128)(2,1)} %copy-done, bf16[1,2048,512]{2,1,0:T(8,128)(2,1)S(1)} %copy-done.2, bf16[1,2048,512]{2,1,0:T(8,128)(2,1)} %expand_ref.1, bf16[1,512,2048]{2,1,0:T(8,128)(2,1)} %contract_ref.1, f32[256,512]{1,0:T(8,128)S(1)} %copy-done.5, ...), custom_call_target="tpu_custom_call" | custom-call | tf_op jit(solution)/shard_map/pallas_call | solution.py:739
  175.0 1.0 copy.26
  (1 shorter events, 0.0 us)
Async XLA Ops:
  58.3 7.0 %copy-start.7 = (s32[256,2]{0,1:T(2,128)S(1)}, s32[256,2]{0,1:T(2,128)}, u32[]{:S(2)}) copy-start(s32[256,2]{0,1:T(2,128)} %param.28) | copy-start | bytes 6148
  58.3 7.2 %copy-start.3 = (bf16[256,2048]{1,0:T(8,128)(2,1)S(1)}, bf16[256,2048]{1,0:T(8,128)(2,1)}, u32[]{:S(2)}) copy-start(bf16[256,2048]{1,0:T(8,128)(2,1)} %skip_ref.1) | copy-start | bytes 3145732
  58.3 7.2 %copy-start.6 = (f32[2048]{0:T(1024)S(1)}, f32[2048]{0:T(1024)}, u32[]{:S(2)}) copy-start(f32[2048]{0:T(1024)} %param.25) | copy-start | bytes 24580
  58.3 63.7 %copy-start.2 = (bf16[1,2048,512]{2,1,0:T(8,128)(2,1)S(1)}, bf16[1,2048,512]{2,1,0:T(8,128)(2,1)}, u32[]{:S(2)}) copy-start(bf16[1,2048,512]{2,1,0:T(8,128)(2,1)} %switch_ref.1) | copy-start | bytes 6291460
  65.4 56.4 %copy-start.8 = (f32[256,2]{0,1:T(2,128)S(1)}, f32[256,2]{0,1:T(2,128)}, u32[]{:S(2)}) copy-start(f32[256,2]{0,1:T(2,128)} %param.27) | copy-start | bytes 6148
  65.4 56.4 %copy-start.9 = (f32[256]{0:T(256)S(1)}, f32[256]{0:T(256)}, u32[]{:S(2)}) copy-start(f32[256]{0:T(256)} %param.26) | copy-start | bytes 3076
  65.5 1.2 copy-start.1
  119.0 1.9 %copy-start = (bf16[8,128,2048]{2,1,0:T(8,128)(2,1)}, bf16[8,128,2048]{2,1,0:T(8,128)(2,1)S(1)}, u32[]{:S(2)}) copy-start(bf16[8,128,2048]{2,1,0:T(8,128)(2,1)S(1)} %get-tuple-element.14.rows_ref) | copy-start | bytes 12582916
  121.0 0.8 copy-start.4
  122.0 1.0 copy-start.5
where the time goes:
time: 179 us; the launch traced here: 176 us
  Pallas kernels  168 us (94%)
  local copies, waits for them, and re-layouts  7.75 us (4%)
    pallas_call x1, Pallas kernels, body(): pl.pallas_call(functools.partial(route_kernel, sp_count, tp_count, expert...  52.2 us
    pallas_call x1, Pallas kernels, body(): pl.pallas_call(functools.partial(return_kernel, sp_count, tp_count), out_...  51.9 us
    pallas_call x1, Pallas kernels, mixer_branch(): pl.pallas_call(functools.partial(mixer_kernel, head_dim, segment), grid=(...  39 us
    pallas_call x1, Pallas kernels, mixer_branch(): pl.pallas_call(functools.partial(exchange_kernel, count, per, workers), o...  17.8 us
    unnamed x23, local copies, waits for them, and re-layouts  7.61 us
    pallas_call x1, Pallas kernels, mixer_branch(): pl.pallas_call(functools.partial(finish_kernel, head_dim), grid=(model_wi...  7 us

commit v1 on v0

--- a/solution.py
+++ b/solution.py
@@ -24,119 +24,186 @@
     return high, (data - high.astype(F32)).astype(BF16)
 
 
-def dot3(left, right, axes=(1, 0)):
-    lh, ll = halves(left)
-    rh, rl = halves(right)
-    return dot(lh, rh, axes) + (dot(lh, rl, axes) + dot(ll, rh, axes))
-
-
-def dot1(left, right, axes=(1, 0)):
-    return dot(left.astype(BF16), right.astype(BF16), axes)
+def stack(*parts):
+    return jnp.concatenate(parts, axis=0)
+
+
+def beside(*parts):
+    return jnp.concatenate(parts, axis=1)
+
+
+def mixer_setup(head_dim, segment, pairs):
+    width = 2 * head_dim
+    row = lax.broadcasted_iota(jnp.int32, (segment, width), 0)
+    lane = lax.broadcasted_iota(jnp.int32, (segment, width), 1)
+    col = lane & (segment - 1)
+    return row, lane, col
+
+
+def split_pair(head_dim):
+    def pick(data):
+        lane = lax.broadcasted_iota(jnp.int32, data.shape, 1)
+        zero = jnp.zeros_like(data)
+        return stack(jnp.where(lane < head_dim, data, zero), jnp.where(lane < head_dim, zero, data))
+
+    return pick
+
+
+def thirds(data):
+    high = data.astype(BF16)
+    rest = data - high.astype(F32)
+    middle = rest.astype(BF16)
+    return high, middle, (rest - middle.astype(F32)).astype(BF16)
+
+
+def mixer_body(head_dim, segment, q_ref, k_ref, v_ref, a_ref, f_ref, b_ref, emit_map, emit_rows):
+    rows, channels = q_ref.shape
+    width = 2 * head_dim
+    pairs = channels // width
+    heads = channels // head_dim
+    blocks = rows // segment
+    shift = segment.bit_length() - 1
+    row, lane, col = mixer_setup(head_dim, segment, pairs)
+    strict, inclusive = row > col, row >= col
+    bd = split_pair(head_dim)
+    own = lax.broadcasted_iota(jnp.int32, (width, width), 0) // head_dim == (
+        lax.broadcasted_iota(jnp.int32, (width, width), 1) // head_dim
+    )
+    ones = jnp.where(own, 1.0, 0.0).astype(BF16)
+    ones = stack(ones, ones)
+    spread = jnp.where(
+        lax.rem(lax.broadcasted_iota(jnp.int32, (3 * heads, channels), 0), heads)
+        == lax.broadcasted_iota(jnp.int32, (3 * heads, channels), 1) // head_dim,
+        1.0,
+        0.0,
+    ).astype(BF16)
+    pieces = stack(*[piece.astype(F32) for piece in thirds(b_ref[...])]).astype(BF16)
+    bias = dot(pieces, spread, (0, 0))
+    t0 = lax.broadcasted_iota(jnp.int32, (segment, segment), 0)
+    t1 = lax.broadcasted_iota(jnp.int32, (segment, segment), 1)
+    triangle = jnp.where(t0 >= t1, 1.0, 0.0).astype(BF16)
+    triangle = beside(triangle, triangle, triangle)
+    chains = [(p, b) for p in range(pairs) for b in range(blocks)]
+
+    def prepare(p, b):
+        at = (slice(b * segment, (b + 1) * segment), slice(p * width, (p + 1) * width))
+        decay = -(0.6065306597126334 / (1.0 + jnp.exp(-f_ref[at]))) + bias[at]
+        cumulative = dot(triangle, stack(*thirds(decay)))
+        keys = k_ref[at].astype(F32)
+        norms = dot(beside(*halves(keys * keys)), ones)
+        removal = keys * lax.rsqrt(norms + 1e-06)
+        beta = removal * (1.0 / (1.0 + jnp.exp(-a_ref[at].astype(F32))))
+        closing = cumulative[segment - 1 :, :]
+        grow = jnp.exp(-cumulative)
+        fade = jnp.exp(closing - cumulative)
+        c = {}
+        c["alpha"] = -removal * jnp.exp(cumulative - decay)
+        c["query"] = q_ref[at].astype(F32) * jnp.exp(cumulative)
+        c["beta_hat"] = beta * grow
+        c["key_hat"] = (keys * grow).astype(BF16)
+        c["beta_bar"] = beta * fade
+        c["key_bar"] = (keys * fade).astype(BF16)
+        c["keep"] = jnp.where(row == col, jnp.exp(closing), 0.0)
+        c["values"] = v_ref[at]
+        return c
+
+    C = [prepare(p, b) for p, b in chains]
+
+    for c in C:
+        ah, al = halves(c["alpha"])
+        bh, bl = halves(c["beta_hat"])
+        qh = c["query"].astype(BF16)
+        by_beta = dot(stack(ah, al, qh), bd(bh), (1, 1))
+        low = dot(ah, bd(bl), (1, 1))
+        by_key = dot(stack(ah, qh), bd(c["key_hat"]), (1, 1))
+        c["lower"] = jnp.where(strict, by_beta[:segment] + by_beta[segment : 2 * segment] + low, 0.0)
+        c["read_remove"] = jnp.where(inclusive, by_beta[2 * segment :], 0.0).astype(BF16)
+        c["remove_write"] = jnp.where(strict, by_key[:segment], 0.0)
+        c["read_write"] = jnp.where(inclusive, by_key[segment:], 0.0).astype(BF16)
+        c["ah"] = ah
+        c["lh"], c["ll"] = halves(c["lower"])
+    for c in C:
+        wh, wl = halves(c["remove_write"])
+        product = dot(stack(wh, wl, c["read_write"]), bd(c["values"]))
+        c["side"] = product[:segment] + product[segment : 2 * segment]
+        c["local"] = product[2 * segment :]
+        c["inverse"] = jnp.where(
+            row == col, 1.0, jnp.where((row >> 1) == (col >> 1), c["lower"], 0.0)
+        )
+    zero = jnp.zeros((segment, width), BF16)
+    for s in range(1, shift):
+        off = ((row >> (s + 1)) == (col >> (s + 1))) & ((row >> s) != (col >> s))
+        for c in C:
+            c["near"] = c["inverse"].astype(BF16)
+            c["reach"] = dot(jnp.where(off, c["lh"], zero), bd(c["near"]))
+        for c in C:
+            c["inverse"] = c["inverse"] + dot(c["near"], bd(c["reach"].astype(BF16)))
+    for c in C:
+        c["near"] = c["inverse"].astype(BF16)
+        c["both"] = beside(c["alpha"], c["side"])
+        c["solved"] = dot(c["near"], beside(bd(c["ah"]), bd(c["side"].astype(BF16))))
+    for c in C:
+        sh, sl = halves(c["solved"])
+        high = dot(stack(c["lh"], c["ll"]), beside(bd(sh[:, :width]), bd(sh[:, width:])))
+        low = dot(c["lh"], beside(bd(sl[:, :width]), bd(sl[:, width:])))
+        c["miss"] = c["both"] - c["solved"] + (high[:segment] + (high[segment:] + low))
+    for c in C:
+        miss = c["miss"].astype(BF16)
+        c["solved"] = c["solved"] + dot(c["near"], beside(bd(miss[:, :width]), bd(miss[:, width:])))
+    for c in C:
+        sh, sl = halves(c["solved"])
+        c["sh"] = sh
+        bh, bl = halves(c["beta_bar"])
+        left = stack(sh, sl, sh, beside(zero, c["values"]))
+        step = dot(left, stack(bh, bh, bl, c["key_bar"]), (0, 0))
+        first = lane < head_dim
+        c["keep"] = c["keep"] + jnp.where(first, step[:head_dim], step[head_dim:width])
+        c["add"] = jnp.where(first, step[width : width + head_dim], step[width + head_dim :])
+    states = [[None] for _ in range(pairs)]
+    now = [stack(C[p * blocks]["keep"], C[p * blocks]["add"]) for p in range(pairs)]
+    for b in range(1, blocks):
+        for p in range(pairs):
+            c = C[p * blocks + b]
+            kh, kl = halves(c["keep"])
+            th, tl = halves(now[p])
+            states[p].append(th)
+            high = dot(stack(th, tl), bd(kh))
+            low = dot(th, bd(kl))
+            total = high[:width] + (high[width:] + low)
+            now[p] = stack(total[:head_dim], total[head_dim:] + c["add"])
+    for p in range(pairs):
+        emit_map(p, now[p])
+    for i, (p, b) in enumerate(chains):
+        c = C[i]
+        sh = c["sh"]
+        read = dot(c["read_remove"], beside(bd(sh[:, :width]), bd(sh[:, width:])))
+        c["read_map"] = c["query"] + read[:, :width]
+        c["local"] = c["local"] + read[:, width:]
+    for i, (p, b) in enumerate(chains):
+        c = C[i]
+        maps, local = c["read_map"].astype(BF16), c["local"]
+        if b:
+            th = states[p][b]
+            seen = dot(maps, stack(bd(th[:head_dim]), bd(th[head_dim:])), (1, 1))
+            maps, local = seen[:, :width].astype(BF16), local + seen[:, width:]
+        emit_rows(p, b, maps, local)
 
 
 def mixer_kernel(head_dim, segment, q_ref, k_ref, v_ref, a_ref, f_ref, b_ref, out_ref, map_ref, ka_ref):
-    pair = pl.program_id(0)
-    rows, width = q_ref.shape
-    blocks = rows // segment
-    per = width // head_dim
-    shift = segment.bit_length() - 1
-    row = lax.broadcasted_iota(jnp.int32, (rows, rows), 0)
-    col = lax.broadcasted_iota(jnp.int32, (rows, rows), 1)
-    same = (row >> shift) == (col >> shift)
-    strict = same & (row > col)
-    inclusive = same & (row >= col)
-    triangle = jnp.where(inclusive, 1.0, 0.0).astype(BF16)
-    lane = lax.broadcasted_iota(jnp.int32, (rows, width), 1)
-    bias = b_ref[...]
-    bias_lane = lax.broadcasted_iota(jnp.int32, bias.shape, 1)
-
-    def spread(values):
-        total = values[per - 1]
-        for h in range(per - 2, -1, -1):
-            total = jnp.where(lane < (h + 1) * head_dim, values[h], total)
-        return total
-
-    own_bias = [
-        jnp.sum(jnp.where(bias_lane == pair * per + h, bias, 0.0), axis=1, keepdims=True)
-        for h in range(per)
-    ]
-    decay = -(0.6065306597126334 / (1.0 + jnp.exp(-f_ref[...]))) + spread(own_bias)
-    high, low = halves(decay)
-    lowest = (decay - high.astype(F32) - low.astype(F32)).astype(BF16)
-    cumulative = dot(triangle, high) + (dot(triangle, low) + dot(triangle, lowest))
-    closing_rows = cumulative.reshape(blocks, segment, width)[:, segment - 1 :, :]
-    closing = jnp.broadcast_to(closing_rows, (blocks, segment, width)).reshape(rows, width)
-    keys = k_ref[...].astype(F32)
-    squares = keys * keys
-    norms = spread(
-        [
-            jnp.sum(squares[:, h * head_dim : (h + 1) * head_dim], axis=1, keepdims=True)
-            for h in range(per)
-        ]
-    )
-    removal = keys * lax.rsqrt(norms + 1e-06)
-    rate = 1.0 / (1.0 + jnp.exp(-a_ref[...].astype(F32)))
-    beta = removal * rate
-    grow = jnp.exp(-cumulative)
-    fade = jnp.exp(closing - cumulative)
-    alpha_all = -removal * jnp.exp(cumulative - decay)
-    beta_hat_all = beta * grow
-    key_hat_all = keys * grow
-    query_all = q_ref[...].astype(F32) * jnp.exp(cumulative)
-    beta_bar_all = beta * fade
-    key_bar_all = keys * fade
-    values_all = v_ref[...]
-    keep_all = jnp.exp(closing_rows)
-    eye = lax.broadcasted_iota(jnp.int32, (head_dim, head_dim), 0) == lax.broadcasted_iota(
-        jnp.int32, (head_dim, head_dim), 1
-    )
-    outs, maps = [], []
-    for h in range(per):
-        part = slice(h * head_dim, (h + 1) * head_dim)
-        alpha, beta_hat, key_hat = alpha_all[:, part], beta_hat_all[:, part], key_hat_all[:, part]
-        query, values = query_all[:, part], values_all[:, part]
-        beta_bar, key_bar = beta_bar_all[:, part], key_bar_all[:, part]
-        lower = jnp.where(strict, dot3(alpha, beta_hat, (1, 1)), 0.0)
-        remove_write = jnp.where(strict, dot1(alpha, key_hat, (1, 1)), 0.0)
-        read_remove = jnp.where(inclusive, dot1(query, beta_hat, (1, 1)), 0.0)
-        read_write = jnp.where(inclusive, dot1(query, key_hat, (1, 1)), 0.0)
-        lh, ll = halves(lower)
-        inverse = jnp.where(row == col, 1.0, jnp.where((row >> 1) == (col >> 1), lower, 0.0))
-        for s in range(1, shift):
-            off = ((row >> (s + 1)) == (col >> (s + 1))) & ((row >> s) != (col >> s))
-            near = inverse.astype(BF16)
-            reach = dot(jnp.where(off, lower, 0.0).astype(BF16), near)
-            inverse = inverse + dot(near, reach.astype(BF16))
-        wh, wl = halves(remove_write)
-        side = jnp.concatenate([alpha, dot(wh, values) + dot(wl, values)], axis=1)
-        near = inverse.astype(BF16)
-        solved = dot(near, side.astype(BF16))
-        sh, sl = halves(solved)
-        miss = side - solved + (dot(lh, sh) + (dot(lh, sl) + dot(ll, sh)))
-        solved = solved + dot(near, miss.astype(BF16))
-        read = dot1(read_remove, solved)
-        read_map = query + read[:, :head_dim]
-        local = read[:, head_dim:] + dot(read_write.astype(BF16), values)
-        state = jnp.concatenate(
-            [jnp.where(eye, 1.0, 0.0), jnp.zeros((head_dim, head_dim), F32)], axis=0
-        )
-        out_rows, map_rows = [], []
-        for b in range(blocks):
-            at = slice(b * segment, (b + 1) * segment)
-            seen = dot1(read_map[at], state, (1, 1))
-            map_rows.append(seen[:, :head_dim])
-            out_rows.append(local[at] + seen[:, head_dim:])
-            step = dot3(solved[at], beta_bar[at], (0, 0))
-            bh, bl = halves(key_bar[at])
-            add = step[head_dim:] + dot(values[at], bh, (0, 0)) + dot(values[at], bl, (0, 0))
-            keep = step[:head_dim] + jnp.where(eye, keep_all[b][:, part], 0.0)
-            state = dot3(state, keep)
-            state = jnp.concatenate([state[:head_dim], state[head_dim:] + add], axis=0)
-        outs.append(jnp.concatenate(out_rows, axis=0))
-        maps.append(jnp.concatenate(map_rows, axis=0))
-        ka_ref[h] = jnp.concatenate([state[:head_dim], state[head_dim:]], axis=1).astype(BF16)
-    out_ref[...] = jnp.concatenate(outs, axis=1)
-    map_ref[...] = jnp.concatenate(maps, axis=1).astype(BF16)
+    width = 2 * head_dim
+
+    def emit_map(p, state):
+        for h in range(2):
+            part = slice(h * head_dim, (h + 1) * head_dim)
+            both = beside(state[:head_dim, part], state[head_dim:, part])
+            ka_ref[2 * p + h] = both.astype(BF16)
+
+    def emit_rows(p, b, maps, local):
+        at = (slice(b * segment, (b + 1) * segment), slice(p * width, (p + 1) * width))
+        out_ref[at] = local
+        map_ref[at] = maps
+
+    mixer_body(head_dim, segment, q_ref, k_ref, v_ref, a_ref, f_ref, b_ref, emit_map, emit_rows)
 
 
 def exchange_kernel(count, per, workers, ka_ref, st_ref, got, fold, send1, recv1, send2, recv2):
@@ -243,23 +310,20 @@
     head_dim = channels // heads
     segment = min(64, rows)
     width = 2 * head_dim
-    pairs = heads // 2
-    block = pl.BlockSpec((rows, width), lambda p: (0, p))
+    vmem = pl.BlockSpec(memory_space=pltpu.VMEM)
     out, maps, ka = pl.pallas_call(
         functools.partial(mixer_kernel, head_dim, segment),
-        grid=(pairs,),
-        in_specs=[block] * 5 + [pl.BlockSpec((rows, heads), lambda p: (0, 0))],
-        out_specs=[block, block, pl.BlockSpec((2, head_dim, width), lambda p: (p, 0, 0))],
+        in_specs=[vmem] * 6,
+        out_specs=[vmem] * 3,
         out_shape=[
             jax.ShapeDtypeStruct((rows, channels), F32),
             jax.ShapeDtypeStruct((rows, channels), BF16),
             jax.ShapeDtypeStruct((heads, head_dim, width), BF16),
         ],
-        compiler_params=pltpu.CompilerParams(vmem_limit_bytes=61 * 1024 * 1024),
-    )(query, key, value, step, forget, bias)
+        compiler_params=pltpu.CompilerParams(vmem_limit_bytes=56 * 1024 * 1024),
+    )(query, key, value, step, forget, bias.T)
     per = max(1, heads // count)
     workers = heads // per
-    vmem = pl.BlockSpec(memory_space=pltpu.VMEM)
     states = pl.pallas_call(
         functools.partial(exchange_kernel, count, per, workers),
         out_shape=jax.ShapeDtypeStruct((heads, head_dim, width), BF16),

time: 179 us -> 146 us (0.82)
  the two profiles are of different devices: /device:TPU:0 before, /device:TPU:11 now
where the time goes in v1:
time: 146 us
  Pallas kernels  140 us (96%)
  local copies, waits for them, and re-layouts  6.26 us (4%)
    pallas_call x1, Pallas kernels, body(): pl.pallas_call(functools.partial(return_kernel, sp_count, tp_count), out_...  57.6 us
    pallas_call x1, Pallas kernels, body(): pl.pallas_call(functools.partial(route_kernel, sp_count, tp_count, expert...  54.1 us
    pallas_call x1, Pallas kernels, mixer_branch(): pl.pallas_call(functools.partial(exchange_kernel, count, per, workers), o...  13.1 us
    pallas_call x1, Pallas kernels, mixer_branch(): pl.pallas_call(functools.partial(mixer_kernel, head_dim, segment), in_spe...  7.73 us
    pallas_call x1, Pallas kernels, mixer_branch(): pl.pallas_call(functools.partial(finish_kernel, head_dim), grid=(model_wi...  7.18 us
    unnamed x22, local copies, waits for them, and re-layouts  6.13 us

profile of v1, /device:TPU:11, one launch (start us, length us, event | category | flops | bytes accessed | tf_op | source)
XLA Modules:
  0.0 146.2 jit_solution(633103704068101346)
XLA Ops:
  0.0 7.7 %shard_map.154 = (f32[256,512]{1,0:T(8,128)}, bf16[256,512]{1,0:T(8,128)(2,1)}, bf16[8,64,128]{2,1,0:T(8,128)(2,1)}) custom-call(bf16[256,512]{1,0:T(8,128)(2,1)} %q_ref.1, bf16[256,512]{1,0:T(8,128)(2,1)} %k_ref.1, bf16[256,512]{1,0:T(8,128)(2,1)} %v_ref.1, bf16[256,512]{1,0:T(8,128)(2,1)} %a_ref.1, f32[256,512]{1,0:T(8,128)} %f_ref.1, f32[8,256]{1,0:T(8,128)} %bitcast.4), custom_call_target="tpu_custom_call" | custom-call | tf_op jit(solution)/shard_map/pallas_call | solution.py:314
  7.7 13.1 %shard_map.155.st_ref = bf16[8,64,128]{2,1,0:T(8,128)(2,1)} custom-call(bf16[8,64,128]{2,1,0:T(8,128)(2,1)} %get-tuple-element.13.ka_ref), custom_call_target="tpu_custom_call" | custom-call | tf_op jit(solution)/shard_map/pallas_call | solution.py:327
  20.8 0.0 copy-start.7
  20.8 0.0 copy-start.3
  20.8 0.0 copy-start.6
  20.8 0.0 copy-start.2
  20.8 7.2 %shard_map.156.part_ref = bf16[256,2048]{1,0:T(8,128)(2,1)} custom-call(f32[256,512]{1,0:T(8,128)} %get-tuple-element.11.out_ref, bf16[256,512]{1,0:T(8,128)(2,1)} %get-tuple-element.12.map_ref, bf16[8,64,128]{2,1,0:T(8,128)(2,1)} %shard_map.155.st_ref, f32[1,512]{1,0:T(1,128)} %bitcast.5, bf16[512,2048]{1,0:T(8,128)(2,1)} %w_ref.1), custom_call_target="tpu_custom_call" | custom-call | tf_op jit(solution)/shard_map/pallas_call | solution.py:345
  28.0 0.0 copy-done.7
  28.0 0.0 copy-start.8
  28.0 0.0 copy-start.9
  28.0 0.1 copy.20.ids_ref
  28.2 0.0 copy-done.3
  28.2 0.0 copy-done.6
  28.2 0.0 copy-start.1
  28.2 1.2 copy-done.1
  29.4 54.1 %shard_map.157 = (f32[256,512]{1,0:T(8,128)S(1)}, s32[256,2]{1,0:T(8,128)S(1)}, bf16[8,128,2048]{2,1,0:T(8,128)(2,1)S(1)}) custom-call(bf16[256,2048]{1,0:T(8,128)(2,1)S(1)} %copy-done.1, bf16[256,2048]{1,0:T(8,128)(2,1)S(1)} %copy-done.3, f32[1,2048]{1,0:T(1,128)S(1)} %bitcast.3, s32[256,2]{1,0:T(8,128)S(1)} %copy.20.ids_ref), custom_call_target="tpu_custom_call" | custom-call | tf_op jit(solution)/shard_map/pallas_call | solution.py:766
  83.6 0.0 copy-start
  83.6 1.9 %copy-done = bf16[8,128,2048]{2,1,0:T(8,128)(2,1)} copy-done((bf16[8,128,2048]{2,1,0:T(8,128)(2,1)}, bf16[8,128,2048]{2,1,0:T(8,128)(2,1)S(1)}, u32[]{:S(2)}) %copy-start) | copy-done | bytes 4194328
  85.5 0.0 copy-start.4
  85.5 0.8 copy-done.4
  86.3 0.0 copy-done.8
  86.3 0.0 copy-done.9
  86.3 0.1 copy.21
  86.5 0.1 broadcast_divide_fusion.weight_ref
  86.6 0.0 copy-done.2
  86.6 0.0 copy-start.5
  86.6 1.0 copy-done.5
  87.6 57.6 %shard_map.158 = bf16[256,2048]{1,0:T(8,128)(2,1)S(1)} custom-call(bf16[8,128,2048]{2,1,0:T(8,128)(2,1)} %copy-done, bf16[1,2048,512]{2,1,0:T(8,128)(2,1)S(1)} %copy-done.2, bf16[1,2048,512]{2,1,0:T(8,128)(2,1)} %expand_ref.1, bf16[1,512,2048]{2,1,0:T(8,128)(2,1)} %contract_ref.1, f32[256,512]{1,0:T(8,128)S(1)} %copy-done.5, ...), custom_call_target="tpu_custom_call" | custom-call | tf_op jit(solution)/shard_map/pallas_call | solution.py:803
  145.2 1.0 copy.24
  (1 shorter events, 0.0 us)
Async XLA Ops:
  20.8 7.2 %copy-start.7 = (s32[256,2]{0,1:T(2,128)S(1)}, s32[256,2]{0,1:T(2,128)}, u32[]{:S(2)}) copy-start(s32[256,2]{0,1:T(2,128)} %param.28) | copy-start | bytes 6148
  20.8 7.4 %copy-start.3 = (bf16[256,2048]{1,0:T(8,128)(2,1)S(1)}, bf16[256,2048]{1,0:T(8,128)(2,1)}, u32[]{:S(2)}) copy-start(bf16[256,2048]{1,0:T(8,128)(2,1)} %skip_ref.1) | copy-start | bytes 3145732
  20.8 7.4 %copy-start.6 = (f32[2048]{0:T(1024)S(1)}, f32[2048]{0:T(1024)}, u32[]{:S(2)}) copy-start(f32[2048]{0:T(1024)} %param.25) | copy-start | bytes 24580
  20.8 65.8 %copy-start.2 = (bf16[1,2048,512]{2,1,0:T(8,128)(2,1)S(1)}, bf16[1,2048,512]{2,1,0:T(8,128)(2,1)}, u32[]{:S(2)}) copy-start(bf16[1,2048,512]{2,1,0:T(8,128)(2,1)} %switch_ref.1) | copy-start | bytes 6291460
  28.0 58.3 %copy-start.8 = (f32[256,2]{0,1:T(2,128)S(1)}, f32[256,2]{0,1:T(2,128)}, u32[]{:S(2)}) copy-start(f32[256,2]{0,1:T(2,128)} %param.27) | copy-start | bytes 6148
  28.0 58.3 %copy-start.9 = (f32[256]{0:T(256)S(1)}, f32[256]{0:T(256)}, u32[]{:S(2)}) copy-start(f32[256]{0:T(256)} %param.26) | copy-start | bytes 3076
  28.2 1.2 copy-start.1
  83.6 1.9 %copy-start = (bf16[8,128,2048]{2,1,0:T(8,128)(2,1)}, bf16[8,128,2048]{2,1,0:T(8,128)(2,1)S(1)}, u32[]{:S(2)}) copy-start(bf16[8,128,2048]{2,1,0:T(8,128)(2,1)S(1)} %get-tuple-element.14.rows_ref) | copy-start | bytes 12582916
  85.5 0.8 copy-start.4
  86.6 1.0 copy-start.5

commit v2 on v1

v2 whole, which is shorter than its diff:
```python
import functools
import math

import jax
import jax.numpy as jnp
from jax import lax
from jax.experimental import pallas as pl
from jax.experimental.pallas import tpu as pltpu
from jax.sharding import PartitionSpec as P

MESH = pl.DeviceIdType.MESH
F32 = jnp.float32
BF16 = jnp.bfloat16
VMEM_LIMIT = 63 * 1024 * 1024


def dot(left, right, axes=(1, 0)):
    return lax.dot_general(
        left, right, (((axes[0],), (axes[1],)), ((), ())), preferred_element_type=F32
    )


def halves(data):
    high = data.astype(BF16)
    return high, (data - high.astype(F32)).astype(BF16)


def stack(*parts):
    return jnp.concatenate(parts, axis=0)


def beside(*parts):
    return jnp.concatenate(parts, axis=1)


def mixer_setup(head_dim, segment, pairs):
    width = 2 * head_dim
    row = lax.broadcasted_iota(jnp.int32, (segment, width), 0)
    lane = lax.broadcasted_iota(jnp.int32, (segment, width), 1)
    col = lane & (segment - 1)
    return row, lane, col


def split_pair(head_dim):
    def pick(data):
        lane = lax.broadcasted_iota(jnp.int32, data.shape, 1)
        zero = jnp.zeros_like(data)
        return stack(jnp.where(lane < head_dim, data, zero), jnp.where(lane < head_dim, zero, data))

    return pick


def thirds(data):
    high = data.astype(BF16)
    rest = data - high.astype(F32)
    middle = rest.astype(BF16)
    return high, middle, (rest - middle.astype(F32)).astype(BF16)


def mixer_body(head_dim, segment, q_ref, k_ref, v_ref, a_ref, f_ref, b_ref, emit_map, between, emit_rows):
    rows, channels = q_ref.shape
    width = 2 * head_dim
    pairs = channels // width
    heads = channels // head_dim
    blocks = rows // segment
    shift = segment.bit_length() - 1
    row, lane, col = mixer_setup(head_dim, segment, pairs)
    strict, inclusive = row > col, row >= col
    bd = split_pair(head_dim)
    own = lax.broadcasted_iota(jnp.int32, (width, width), 0) // head_dim == (
        lax.broadcasted_iota(jnp.int32, (width, width), 1) // head_dim
    )
    ones = jnp.where(own, 1.0, 0.0).astype(BF16)
    ones = stack(ones, ones)
    spread = jnp.where(
        lax.rem(lax.broadcasted_iota(jnp.int32, (3 * heads, channels), 0), heads)
        == lax.broadcasted_iota(jnp.int32, (3 * heads, channels), 1) // head_dim,
        1.0,
        0.0,
    ).astype(BF16)
    pieces = stack(*[piece.astype(F32) for piece in thirds(b_ref[...])]).astype(BF16)
    bias = dot(pieces, spread, (0, 0))
    t0 = lax.broadcasted_iota(jnp.int32, (segment, segment), 0)
    t1 = lax.broadcasted_iota(jnp.int32, (segment, segment), 1)
    triangle = jnp.where(t0 >= t1, 1.0, 0.0).astype(BF16)
    triangle = beside(triangle, triangle, triangle)
    chains = [(p, b) for p in range(pairs) for b in range(blocks)]

    def prepare(p, b):
        at = (slice(b * segment, (b + 1) * segment), slice(p * width, (p + 1) * width))
        decay = -(0.6065306597126334 / (1.0 + jnp.exp(-f_ref[at]))) + bias[at]
        cumulative = dot(triangle, stack(*thirds(decay)))
        keys = k_ref[at].astype(F32)
        norms = dot(beside(*halves(keys * keys)), ones)
        removal = keys * lax.rsqrt(norms + 1e-06)
        beta = removal * (1.0 / (1.0 + jnp.exp(-a_ref[at].astype(F32))))
        closing = cumulative[segment - 1 :, :]
        grow = jnp.exp(-cumulative)
        fade = jnp.exp(closing - cumulative)
        c = {}
        c["alpha"] = -removal * jnp.exp(cumulative - decay)
        c["query"] = q_ref[at].astype(F32) * jnp.exp(cumulative)
        c["beta_hat"] = beta * grow
        c["key_hat"] = (keys * grow).astype(BF16)
        c["beta_bar"] = beta * fade
        c["key_bar"] = (keys * fade).astype(BF16)
        c["keep"] = jnp.where(row == col, jnp.exp(closing), 0.0)
        c["values"] = v_ref[at]
        return c

    C = [prepare(p, b) for p, b in chains]

    for c in C:
        ah, al = halves(c["alpha"])
        bh, bl = halves(c["beta_hat"])
        qh = c["query"].astype(BF16)
        by_beta = dot(stack(ah, al, qh), bd(bh), (1, 1))
        low = dot(ah, bd(bl), (1, 1))
        by_key = dot(stack(ah, qh), bd(c["key_hat"]), (1, 1))
        c["lower"] = jnp.where(strict, by_beta[:segment] + by_beta[segment : 2 * segment] + low, 0.0)
        c["read_remove"] = jnp.where(inclusive, by_beta[2 * segment :], 0.0).astype(BF16)
        c["remove_write"] = jnp.where(strict, by_key[:segment], 0.0)
        c["read_write"] = jnp.where(inclusive, by_key[segment:], 0.0).astype(BF16)
        c["ah"] = ah
        c["lh"], c["ll"] = halves(c["lower"])
    for c in C:
        wh, wl = halves(c["remove_write"])
        product = dot(stack(wh, wl, c["read_write"]), bd(c["values"]))
        c["side"] = product[:segment] + product[segment : 2 * segment]
        c["local"] = product[2 * segment :]
        c["inverse"] = jnp.where(
            row == col, 1.0, jnp.where((row >> 1) == (col >> 1), c["lower"], 0.0)
        )
    zero = jnp.zeros((segment, width), BF16)
    for s in range(1, shift):
        off = ((row >> (s + 1)) == (col >> (s + 1))) & ((row >> s) != (col >> s))
        for c in C:
            c["near"] = c["inverse"].astype(BF16)
            c["reach"] = dot(jnp.where(off, c["lh"], zero), bd(c["near"]))
        for c in C:
            c["inverse"] = c["inverse"] + dot(c["near"], bd(c["reach"].astype(BF16)))
    for c in C:
        c["near"] = c["inverse"].astype(BF16)
        c["both"] = beside(c["alpha"], c["side"])
        c["solved"] = dot(c["near"], beside(bd(c["ah"]), bd(c["side"].astype(BF16))))
    for c in C:
        sh, sl = halves(c["solved"])
        high = dot(stack(c["lh"], c["ll"]), beside(bd(sh[:, :width]), bd(sh[:, width:])))
        low = dot(c["lh"], beside(bd(sl[:, :width]), bd(sl[:, width:])))
        c["miss"] = c["both"] - c["solved"] + (high[:segment] + (high[segment:] + low))
    for c in C:
        miss = c["miss"].astype(BF16)
        c["solved"] = c["solved"] + dot(c["near"], beside(bd(miss[:, :width]), bd(miss[:, width:])))
    for c in C:
        sh, sl = halves(c["solved"])
        c["sh"] = sh
        bh, bl = halves(c["beta_bar"])
        left = stack(sh, sl, sh, beside(zero, c["values"]))
        step = dot(left, stack(bh, bh, bl, c["key_bar"]), (0, 0))
        first = lane < head_dim
        c["keep"] = c["keep"] + jnp.where(first, step[:head_dim], step[head_dim:width])
        c["add"] = jnp.where(first, step[width : width + head_dim], step[width + head_dim :])
    states = [[None] for _ in range(pairs)]
    now = [stack(C[p * blocks]["keep"], C[p * blocks]["add"]) for p in range(pairs)]
    for b in range(1, blocks):
        for p in range(pairs):
            c = C[p * blocks + b]
            kh, kl = halves(c["keep"])
            th, tl = halves(now[p])
            states[p].append(th)
            high = dot(stack(th, tl), bd(kh))
            low = dot(th, bd(kl))
            total = high[:width] + (high[width:] + low)
            now[p] = stack(total[:head_dim], total[head_dim:] + c["add"])
    for p in range(pairs):
        emit_map(p, now[p])
    between()
    for i, (p, b) in enumerate(chains):
        c = C[i]
        sh = c["sh"]
        read = dot(c["read_remove"], beside(bd(sh[:, :width]), bd(sh[:, width:])))
        c["read_map"] = c["query"] + read[:, :width]
        c["local"] = c["local"] + read[:, width:]
    for i, (p, b) in enumerate(chains):
        c = C[i]
        maps, local = c["read_map"].astype(BF16), c["local"]
        if b:
            th = states[p][b]
            seen = dot(maps, stack(bd(th[:head_dim]), bd(th[head_dim:])), (1, 1))
            maps, local = seen[:, :width].astype(BF16), local + seen[:, width:]
        emit_rows(p, b, maps, local)


def mate(me, d, count):
    total, bit = 0, 1
    while bit < count:
        own = lax.rem(lax.div(me, bit), 2)
        total = total + bit * (1 - own if d & bit else own)
        bit *= 2
    return total


def call_peers(sp_count, tp_count, sp, tp):
    barrier = pltpu.get_barrier_semaphore()
    for d in range(1, sp_count):
        pl.semaphore_signal(
            barrier, inc=1, device_id={"sp": lax.rem(sp + d, sp_count)}, device_id_type=MESH
        )
    for d in range(1, tp_count):
        pl.semaphore_signal(
            barrier, inc=1, device_id={"tp": lax.rem(tp + d, tp_count)}, device_id_type=MESH
        )


def meet_peers(sp_count, tp_count):
    pl.semaphore_wait(pltpu.get_barrier_semaphore(), sp_count + tp_count - 2)


def copy_to(src, dst, send, recv, device):
    return pltpu.make_async_remote_copy(
        src_ref=src,
        dst_ref=dst,
        send_sem=send,
        recv_sem=recv,
        device_id=device,
        device_id_type=MESH,
    )


def span(index, size):
    return pl.ds(pl.multiple_of(index * size, size), size)


def row_total(data, terms):
    ones = jnp.ones((8, data.shape[1]), BF16)
    total = None
    for _ in range(terms):
        piece = data.astype(BF16)
        data = data - piece.astype(F32)
        product = dot(ones, piece, (1, 1))
        total = product if total is None else total + product
    return total


def back(
    sp_count, tp_count, ready,
    rows_ref, switch_ref, expand_ref, contract_ref, hidden_ref, slots, weight_ref, out_ref,
    y_ref, from_sib, pair, from_peer, summed, back,
    s_sib, r_sib, s_peer, r_peer, s_back, r_back, s_own, s_fwd, r_col,
):
    sp, tp = lax.axis_index("sp"), lax.axis_index("tp")
    per, model = y_ref.shape[1:]
    rows = hidden_ref.shape[0]
    cols = model // tp_count
    mine = span(tp, cols)
    groups = tp_count // 2
    core, group = lax.rem(tp, 2), tp // 2
    sibling = group * 2 + 1 - core

    def sib_copy(s, g):
        return copy_to(
            y_ref.at[s, :, span(g * 2 + 1 - core, cols)],
            from_sib.at[s, g],
            s_sib.at[s, g],
            r_sib.at[s, g],
            {"tp": sibling},
        )

    def peer_copy(s, g):
        return copy_to(
            pair.at[s, g],
            from_peer.at[s, group],
            s_peer.at[s, g],
            r_peer.at[s, group],
            {"tp": g * 2 + core},
        )

    def back_copy(t):
        return copy_to(summed.at[t], back.at[sp], s_back.at[t], r_back.at[sp], {"sp": t})

    def others():
        return [lax.rem(group + d, groups) for d in range(1, groups)]

    local = switch_ref.shape[0]
    capacity = per // local
    chunk = math.gcd(sp_count, max(1, 256 // capacity))
    chunks = sp_count // chunk
    half = sp_count // 2
    ranks = list(range(half, sp_count)) + list(range(half - 1, -1, -1))
    order = [mate(sp, d, sp_count) for d in ranks]

    def expert(at):
        for s in at:
            ready(s)
        for e in range(local):
            inside = slice(e * capacity, (e + 1) * capacity)
            data = jnp.concatenate([rows_ref[s, inside, :] for s in at], axis=0)
            gate = dot(data, switch_ref[e])
            units = (gate / (1.0 + jnp.exp(-gate)) * dot(data, expand_ref[e])).astype(BF16)
            value = dot(units, contract_ref[e]).astype(BF16)
            for c in range(chunk):
                y_ref[at[c], inside, :] = value[c * capacity : (c + 1) * capacity]
        for s in at:
            for g in others():
                sib_copy(s, g).start()
            sib_copy(s, group).start()

    def meet(s):
        for g in others():
            sib_copy(s, g).wait_recv()
            pair[s, g] = (
                y_ref[s, :, span(g * 2 + core, cols)].astype(F32) + from_sib[s, g].astype(F32)
            ).astype(BF16)
            peer_copy(s, g).start()

    def total_up(s, own):
        sib_copy(s, group).wait_recv()
        total = y_ref[s, :, mine].astype(F32) + from_sib[s, group].astype(F32)
        for g in others():
            copy_to(
                from_peer.at[s, g],
                from_peer.at[s, g],
                s_peer.at[s, g],
                r_peer.at[s, g],
                {"tp": g * 2 + core},
            ).wait_recv()
            total = total + from_peer[s, g].astype(F32)
        if own:
            back[s] = total.astype(BF16)
        else:
            summed[s] = total.astype(BF16)
            back_copy(s).start()

    for i in range(chunks + 1):
        if i < chunks:
            at = order[i * chunk : (i + 1) * chunk]
            expert(at)
            for s in at:
                meet(s)
        if i:
            for c in range((i - 1) * chunk, i * chunk):
                total_up(order[c], ranks[c] == 0)
    weights = weight_ref[...]
    places = lax.broadcasted_iota(jnp.int32, (rows, per), 1)
    top = len(slots)
    result = hidden_ref[...]
    landing = ranks[: half - 1] + ranks[half:] + [ranks[half - 1]]
    for d in landing:
        s = mate(sp, d, sp_count)
        if d:
            copy_to(back.at[s], back.at[s], s_back.at[s], r_back.at[s], {"sp": s}).wait_recv()
        chosen = [
            jnp.where(slots[k] == places + s * per, 1.0, 0.0).astype(BF16)
            for k in range(top)
        ]
        picked = dot(stack(*chosen), back[s])
        for k in range(top):
            result = result + weights[:, k : k + 1] * picked[k * rows : (k + 1) * rows]
    out_ref[:, mine] = result.astype(BF16)

    def own_copy(p):
        here = out_ref.at[:, mine]
        return copy_to(here, here, s_own.at[p], r_col.at[tp], {"tp": p})

    def forward(o):
        here = out_ref.at[:, span(o, cols)]
        return copy_to(here, here, s_fwd.at[o], r_col.at[o], {"tp": sibling})

    peers = [g * 2 + core for g in others()]
    for p in peers:
        own_copy(p).start()
    own_copy(sibling).start()
    for p in peers:
        forward(p).wait_recv()
        forward(p).start()
    forward(sibling).wait_recv()
    for g in others():
        forward(g * 2 + 1 - core).wait_recv()
    own_copy(sibling).wait_send()
    for p in peers:
        own_copy(p).wait_send()
        forward(p).wait_send()

    def close(s, carry):
        sib_copy(s, group).wait_send()
        for g in others():
            sib_copy(s, g).wait_send()
            peer_copy(s, g).wait_send()
        return carry

    lax.fori_loop(0, sp_count, close, 0)

    def sent(d, carry):
        back_copy(lax.rem(sp + d, sp_count)).wait_send()
        return carry

    lax.fori_loop(1, sp_count, sent, 0)


def layer_kernel(
    head_dim, segment, sp_count, tp_count, experts, capacity,
    q_in, k_in, v_in, a_in, f_in, b_in, w_in, skip_in, switch_in, expand_in, contract_in,
    norm_ref, gain_ref, ids_ref, weight_ref,
    out_ref,
    q_ref, k_ref, v_ref, a_ref, f_ref, b_ref, w_ref, skip_ref, s_in,
    local, maps_in, ka, got, fold, st, mixed,
    lent, kept, from_sib, pair, from_peer, squares, outgoing,
    s_map, r_map, s_fold, r_fold, s_sib, r_sib, s_peer, r_peer,
    s_sq, r_sq, s_out, r_out, s_own, s_fwd, r_col,
    hidden_ref, rows_ref, switch_ref, expand_ref, contract_ref, *back_refs,
):
    sp, tp = lax.axis_index("sp"), lax.axis_index("tp")
    rows, channels = q_in.shape
    model = skip_in.shape[1]
    cols = model // tp_count
    width = 2 * head_dim
    heads = channels // head_dim
    share = max(1, heads // sp_count)
    workers = heads // share
    mine = span(tp, cols)
    groups = tp_count // 2
    core, group = lax.rem(tp, 2), lax.div(tp, 2)
    sibling = group * 2 + 1 - core
    others = [lax.rem(group + g, groups) for g in range(1, groups)]
    early = [
        pltpu.make_async_copy(src, dst, s_in.at[i])
        for i, (src, dst) in enumerate(
            [(f_in, f_ref), (b_in, b_ref), (k_in, k_ref), (a_in, a_ref), (q_in, q_ref),
             (v_in, v_ref), (w_in, w_ref), (skip_in, skip_ref), (switch_in, switch_ref),
             (expand_in, expand_ref), (contract_in, contract_ref)]
        )
    ]
    for copy in early:
        copy.start()
    call_peers(sp_count, tp_count, sp, tp)
    for copy in early[:6]:
        copy.wait()

    def unless_me(t, action):
        pl.when(t != sp)(action)

    def map_copy(t, owner):
        return copy_to(
            ka.at[pl.ds(t * share, share)], got.at[owner], s_map.at[t], r_map.at[owner], {"sp": t}
        )

    def fold_copy(t, owner):
        return copy_to(
            fold.at[t], st.at[pl.ds(owner * share, share)], s_fold.at[t], r_fold.at[owner], {"sp": t}
        )

    def emit_map(p, state):
        for h in range(2):
            part = slice(h * head_dim, (h + 1) * head_dim)
            ka[2 * p + h] = beside(state[:head_dim, part], state[head_dim:, part]).astype(BF16)

    def send_maps():
        meet_peers(sp_count, tp_count)
        if workers == sp_count:
            for d in range(1, sp_count):
                map_copy(mate(sp, d, sp_count), sp).start()
        else:
            for t in range(workers):
                unless_me(t, lambda t=t: map_copy(t, sp).start())

    def emit_rows(p, b, maps, out):
        at = (slice(b * segment, (b + 1) * segment), slice(p * width, (p + 1) * width))
        local[at] = out
        maps_in[at] = maps

    mixer_body(
        head_dim, segment, q_ref, k_ref, v_ref, a_ref, f_ref, b_ref, emit_map, send_maps, emit_rows
    )

    ids = ids_ref[...]
    top = ids.shape[1]
    lanes = lax.broadcasted_iota(jnp.int32, (rows, experts), 1)
    named = [ids[:, k : k + 1] == lanes for k in range(top)]
    anyone = sum(jnp.where(n, 1.0, 0.0) for n in named).astype(BF16)
    r0 = lax.broadcasted_iota(jnp.int32, (rows, rows), 0)
    r1 = lax.broadcasted_iota(jnp.int32, (rows, rows), 1)
    before = dot(jnp.where(r0 > r1, 1.0, 0.0).astype(BF16), anyone)
    slots = [
        jnp.sum(
            jnp.where(n, before + lanes.astype(F32) * capacity, 0.0), axis=1, keepdims=True
        ).astype(jnp.int32)
        for n in named
    ]
    def chain():
        got[sp] = ka[pl.ds(sp * share, share)]
        half = lax.div(lax.broadcasted_iota(jnp.int32, (head_dim, width), 1), head_dim)
        places = [half == lax.rem(sp * share + i, 2) for i in range(share)]
        state = [jnp.zeros((head_dim, head_dim), F32) for _ in range(share)]
        for j in range(sp_count):
            unless_me(
                j,
                lambda j=j: copy_to(
                    got.at[j], got.at[j], s_map.at[0], r_map.at[j], {"sp": j}
                ).wait_recv(),
            )
            for i in range(share):
                fold[j, i] = jnp.where(places[i], beside(state[i], state[i]), 0.0).astype(BF16)
            unless_me(j, lambda j=j: fold_copy(j, sp).start())
            for i in range(share):
                both = got[j, i]
                product = dot(stack(*halves(state[i])), both[:, :head_dim])
                state[i] = product[:head_dim] + product[head_dim:] + both[:, head_dim:].astype(F32)
        st[pl.ds(sp * share, share)] = fold[sp]

    if workers == sp_count:
        chain()
    else:
        pl.when(sp < workers)(chain)
    ones = jnp.where(
        lax.div(lax.broadcasted_iota(jnp.int32, (width, width), 0), head_dim)
        == lax.div(lax.broadcasted_iota(jnp.int32, (width, width), 1), head_dim),
        1.0 / head_dim,
        0.0,
    ).astype(BF16)
    ones = stack(ones, ones)
    for t in range(workers):
        unless_me(
            t,
            lambda t=t: copy_to(
                fold.at[t], st.at[pl.ds(t * share, share)], s_fold.at[0], r_fold.at[t], {"sp": t}
            ).wait_recv(),
        )
    for p in range(heads // 2):
        part = slice(p * width, (p + 1) * width)
        states = stack(st[2 * p], st[2 * p + 1])
        output = local[:, part] + dot(maps_in[:, part], states, (1, 1))
        centered = output - dot(beside(*halves(output)), ones)
        spread = dot(beside(*halves(centered * centered)), ones)
        mixed[:, part] = (centered * lax.rsqrt(spread + 0.00064) * norm_ref[:, part]).astype(BF16)

    def sib_copy(g):
        return copy_to(lent.at[g], from_sib.at[g], s_sib.at[g], r_sib.at[g], {"tp": sibling})

    def peer_copy(g):
        return copy_to(
            pair.at[g], from_peer.at[group], s_peer.at[g], r_peer.at[group], {"tp": g * 2 + core}
        )

    for copy in early[6:8]:
        copy.wait()
    for g in others + [group]:
        lent[g] = dot(mixed[...], w_ref[:, span(g * 2 + 1 - core, cols)]).astype(BF16)
        sib_copy(g).start()
    for g in others + [group]:
        kept[g] = dot(mixed[...], w_ref[:, span(g * 2 + core, cols)])
    for g in others:
        sib_copy(g).wait_recv()
        pair[g] = (kept[g] + from_sib[g].astype(F32)).astype(BF16)
        peer_copy(g).start()
    sib_copy(group).wait_recv()
    hidden = skip_ref[:, mine].astype(F32) + (kept[group] + from_sib[group].astype(F32))
    for g in others:
        copy_to(
            pair.at[g], from_peer.at[g], s_peer.at[g], r_peer.at[g], {"tp": g * 2 + core}
        ).wait_recv()
        hidden = hidden + from_peer[g].astype(F32)
    hidden_ref[...] = hidden
    squares[tp] = row_total(hidden * hidden, 3)

    def square_copy(p):
        return copy_to(squares.at[tp], squares.at[tp], s_sq.at[p], r_sq.at[tp], {"tp": p})

    for d in range(1, tp_count):
        square_copy(lax.rem(tp + d, tp_count)).start()
    total = squares[tp]
    for d in range(1, tp_count):
        p = lax.rem(tp + d, tp_count)
        copy_to(squares.at[p], squares.at[p], s_sq.at[p], r_sq.at[p], {"tp": p}).wait_recv()
        total = total + squares[p]
    inverse = lax.rsqrt(total / model + 1e-06)
    first = jnp.where(lax.broadcasted_iota(jnp.int32, (8, 128), 0) == 0, 1.0, 0.0).astype(BF16)
    column = None
    for _ in range(3):
        piece = inverse.astype(BF16)
        inverse = inverse - piece.astype(F32)
        product = dot(piece, first, (0, 0))
        column = product if column is None else column + product
    normed = (hidden * column[:, :1] * gain_ref[:, mine]).astype(BF16)

    per = experts // sp_count * capacity
    places = lax.broadcasted_iota(jnp.int32, (rows, per), 1)

    def block_for(t):
        at = places + t * per
        chosen = slots[0] == at
        for s in slots[1:]:
            chosen = chosen | (s == at)
        return dot(jnp.where(chosen, 1.0, 0.0).astype(BF16), normed, (0, 0)).astype(BF16)

    def out_copy(t):
        return copy_to(
            outgoing.at[t], rows_ref.at[sp, :, mine], s_out.at[t], r_out.at[sp], {"sp": t}
        )

    def own_copy(p, s):
        here = rows_ref.at[s, :, mine]
        return copy_to(here, here, s_own.at[p, s], r_col.at[tp, s], {"tp": p})

    def forward(o, s):
        here = rows_ref.at[s, :, span(o, cols)]
        return copy_to(here, here, s_fwd.at[o, s], r_col.at[o, s], {"tp": sibling})

    peers = [g * 2 + core for g in others]

    def pass_on(s):
        for p in peers:
            own_copy(p, s).start()
        own_copy(sibling, s).start()

    near, far = list(range(1, sp_count // 2)), list(range(sp_count // 2, sp_count))
    sending, landing = [], [0]
    for i, d in enumerate(far):
        sending += near[i : i + 1] + [d]
    landing = [0] + near[:2] + sum([[d] + near[i + 2 : i + 3] for i, d in enumerate(far)], [])
    for d in sending[:2]:
        outgoing[mate(sp, d, sp_count)] = block_for(mate(sp, d, sp_count))
        out_copy(mate(sp, d, sp_count)).start()
    rows_ref[sp, :, mine] = block_for(sp)
    pass_on(sp)
    for d in sending[2:]:
        outgoing[mate(sp, d, sp_count)] = block_for(mate(sp, d, sp_count))
        out_copy(mate(sp, d, sp_count)).start()
    lag = 2

    def relay(i):
        if i < sp_count:
            s = mate(sp, landing[i], sp_count)
            here = rows_ref.at[s, :, mine]
            copy_to(here, here, s_out.at[s], r_out.at[s], {"sp": s}).wait_recv()
            pass_on(s)
        if i >= lag:
            s = mate(sp, landing[i - lag], sp_count)
            for o in peers:
                forward(o, s).wait_recv()
                forward(o, s).start()

    def ready(s):
        forward(sibling, s).wait_recv()
        for g in others:
            forward(g * 2 + 1 - core, s).wait_recv()

    for i in range(1, sp_count + lag):
        relay(i)
    for copy in early[8:]:
        copy.wait()
    back(
        sp_count, tp_count, ready,
        rows_ref, switch_ref, expand_ref, contract_ref, hidden_ref, slots, weight_ref, out_ref,
        *back_refs,
    )

    def settle(s, carry):
        own_copy(sibling, s).wait_send()
        for p in peers:
            own_copy(p, s).wait_send()
            forward(p, s).wait_send()
        return carry

    lax.fori_loop(0, sp_count, settle, 0)

    def sent(d, carry):
        out_copy(lax.rem(sp + d, sp_count)).wait_send()
        return carry

    lax.fori_loop(1, sp_count, sent, 0)
    for d in range(1, tp_count):
        square_copy(lax.rem(tp + d, tp_count)).wait_send()
    for g in others:
        sib_copy(g).wait_send()
        peer_copy(g).wait_send()
    sib_copy(group).wait_send()
    for t in range(workers):
        unless_me(t, lambda t=t: map_copy(t, sp).wait_send())

    def folded():
        for t in range(sp_count):
            unless_me(t, lambda t=t: fold_copy(t, sp).wait_send())

    if workers == sp_count:
        folded()
    else:
        pl.when(sp < workers)(folded)


def body(
    readout_query_vectors,
    attention_key_vectors,
    attention_content_vectors,
    step_size_preactivation,
    forgetting_preactivation,
    extra_forgetting_bias,
    subspace_normalizer_gain,
    skip_connection_stream,
    blender_projection_matrix,
    specialist_prenormal_gain,
    cluster_router_chance,
    specialist_chance_within_cluster,
    chosen_specialist_ids,
    specialist_switch_matrix,
    specialist_expansion_matrix,
    specialist_contraction_matrix,
):
    tok_rows, model_width = skip_connection_stream.shape
    sp_count, tp_count = lax.axis_size("sp"), lax.axis_size("tp")
    local_experts = specialist_switch_matrix.shape[0]
    experts = local_experts * sp_count
    top_count = chosen_specialist_ids.shape[1]
    capacity = 2 * tok_rows * top_count // experts
    cols = model_width // tp_count
    per = local_experts * capacity
    groups = tp_count // 2
    channels = readout_query_vectors.shape[1]
    heads = extra_forgetting_bias.shape[1]
    head_dim = channels // heads
    share = max(1, heads // sp_count)
    vmem = pl.BlockSpec(memory_space=pltpu.VMEM)
    hbm = pl.BlockSpec(memory_space=pltpu.HBM)
    sems = pltpu.SemaphoreType.DMA
    route_weight = (
        cluster_router_chance[:, None]
        * specialist_chance_within_cluster
        / jnp.sum(specialist_chance_within_cluster, axis=1, keepdims=True)
    )
    return pl.pallas_call(
        functools.partial(
            layer_kernel, head_dim, min(64, tok_rows), sp_count, tp_count, experts, capacity
        ),
        out_shape=jax.ShapeDtypeStruct((tok_rows, model_width), BF16),
        in_specs=[hbm] * 11 + [vmem] * 4,
        out_specs=vmem,
        scratch_shapes=[
            pltpu.VMEM((tok_rows, channels), BF16),
            pltpu.VMEM((tok_rows, channels), BF16),
            pltpu.VMEM((tok_rows, channels), BF16),
            pltpu.VMEM((tok_rows, channels), BF16),
            pltpu.VMEM((tok_rows, channels), F32),
            pltpu.VMEM((heads, tok_rows), F32),
            pltpu.VMEM((channels, model_width), BF16),
            pltpu.VMEM((tok_rows, model_width), BF16),
            sems((11,)),
            pltpu.VMEM((tok_rows, channels), F32),
            pltpu.VMEM((tok_rows, channels), BF16),
            pltpu.VMEM((heads, head_dim, 2 * head_dim), BF16),
            pltpu.VMEM((sp_count, share, head_dim, 2 * head_dim), BF16),
            pltpu.VMEM((sp_count, share, head_dim, 2 * head_dim), BF16),
            pltpu.VMEM((heads, head_dim, 2 * head_dim), BF16),
            pltpu.VMEM((tok_rows, channels), BF16),
            pltpu.VMEM((groups, tok_rows, cols), BF16),
            pltpu.VMEM((groups, tok_rows, cols), F32),
            pltpu.VMEM((groups, tok_rows, cols), BF16),
            pltpu.VMEM((groups, tok_rows, cols), BF16),
            pltpu.VMEM((groups, tok_rows, cols), BF16),
            pltpu.VMEM((tp_count, 8, tok_rows), F32),
            pltpu.VMEM((sp_count, per, cols), BF16),
            sems((sp_count,)),
            sems((sp_count,)),
            sems((sp_count,)),
            sems((sp_count,)),
            sems((groups,)),
            sems((groups,)),
            sems((groups,)),
            sems((groups,)),
            sems((tp_count,)),
            sems((tp_count,)),
            sems((sp_count,)),
            sems((sp_count,)),
            sems((tp_count, sp_count)),
            sems((tp_count, sp_count)),
            sems((tp_count, sp_count)),
            pltpu.VMEM((tok_rows, cols), F32),
            pltpu.VMEM((sp_count, per, model_width), BF16),
            pltpu.VMEM(specialist_switch_matrix.shape, BF16),
            pltpu.VMEM(specialist_expansion_matrix.shape, BF16),
            pltpu.VMEM(specialist_contraction_matrix.shape, BF16),
            pltpu.VMEM((sp_count, per, model_width), BF16),
            pltpu.VMEM((sp_count, groups, per, cols), BF16),
            pltpu.VMEM((sp_count, groups, per, cols), BF16),
            pltpu.VMEM((sp_count, groups, per, cols), BF16),
            pltpu.VMEM((sp_count, per, cols), BF16),
            pltpu.VMEM((sp_count, per, cols), BF16),
            sems((sp_count, groups)),
            sems((sp_count, groups)),
            sems((sp_count, groups)),
            sems((sp_count, groups)),
            sems((sp_count,)),
            sems((sp_count,)),
            sems((tp_count,)),
            sems((tp_count,)),
            sems((tp_count,)),
        ],
        compiler_params=pltpu.CompilerParams(
            collective_id=1, has_side_effects=True, vmem_limit_bytes=VMEM_LIMIT
        ),
    )(
        readout_query_vectors,
        attention_key_vectors,
        attention_content_vectors,
        step_size_preactivation,
        forgetting_preactivation,
        extra_forgetting_bias.T,
        blender_projection_matrix,
        skip_connection_stream,
        specialist_switch_matrix,
        specialist_expansion_matrix,
        specialist_contraction_matrix,
        subspace_normalizer_gain.reshape(1, channels),
        specialist_prenormal_gain.reshape(1, model_width),
        chosen_specialist_ids,
        route_weight,
    )


def solution(mesh):
    in_specs = (
        P("sp", "tp"),
        P("sp", "tp"),
        P("sp", "tp"),
        P("sp", "tp"),
        P("sp", "tp"),
        P("sp", "tp"),
        P("tp"),
        P("sp", None),
        P("tp", None),
        P(),
        P("sp"),
        P("sp", None),
        P("sp", None),
        P("sp", None, "tp"),
        P("sp", None, "tp"),
        P("sp", "tp", None),
    )
    out_specs = P("sp", None)
    return jax.shard_map(body, mesh=mesh, in_specs=in_specs, out_specs=out_specs, check_vma=False)
```

time: 146 us -> 113 us (0.77)
  the two profiles are of different devices: /device:TPU:11 before, /device:TPU:0 now
where the time goes in v2:
time: 113 us
  Pallas kernels  107 us (95%)
  local copies, waits for them, and re-layouts  3.91 us (3%)
  other arithmetic  1.47 us (1%)
    pallas_call x1, Pallas kernels, body(): pl.pallas_call(functools.partial(layer_kernel, head_dim, min(64, tok_rows...  107 us
    unnamed x2, local copies, waits for them, and re-layouts  3.78 us

profile of v2, /device:TPU:0, one launch (start us, length us, event | category | flops | bytes accessed | tf_op | source)
XLA Modules:
  0.0 112.6 jit_solution(2294772751696281777)
XLA Ops:
  0.0 0.7 fusion
  0.7 0.1 copy.20
  0.9 0.8 broadcast_divide_fusion.weight_ref
  1.6 1.5 %copy.22.ids_ref = s32[256,2]{1,0:T(8,128)} copy(s32[256,2]{0,1:T(2,128)} %param.28) | data formatting | bytes 4096 | tf_op args[12]
  3.1 107.2 %shard_map.154 = bf16[256,2048]{1,0:T(8,128)(2,1)} custom-call(bf16[256,512]{1,0:T(8,128)(2,1)} %q_in.1, bf16[256,512]{1,0:T(8,128)(2,1)} %k_in.1, bf16[256,512]{1,0:T(8,128)(2,1)} %v_in.1, bf16[256,512]{1,0:T(8,128)(2,1)} %a_in.1, f32[256,512]{1,0:T(8,128)} %f_in.1, f32[8,256]{1,0:T(8,128)} %bitcast.3, bf16[512,2048]{1,0:T(8,128)(2,1)} %w_in.1, ...), custom_call_target="tpu_custom_call" | custom-call | tf_op jit(solution)/shard_map/pallas_call | solution.py:729
  110.3 2.3 %copy.24 = bf16[256,2048]{1,0:T(8,128)(2,1)} copy(bf16[256,2048]{1,0:T(8,128)(2,1)} %shard_map.154) | data formatting | bytes 2097152

commit v3 on v2

--- a/solution.py
+++ b/solution.py
@@ -12,6 +12,15 @@
 F32 = jnp.float32
 BF16 = jnp.bfloat16
 VMEM_LIMIT = 63 * 1024 * 1024
+SENDS = [6, 1, 5, 2, 3, 4, 7]
+SCRIPT = [
+    ("R", 1), ("R", 0), ("R", 6), ("R", 5), ("R", 2), ("R", 3), ("F", 5), ("F", 0), ("F", 2),
+    ("R", 4), ("E", 2, 5), ("F", 3), ("M", 5), ("E", 3), ("F", 1), ("F", 4), ("R", 7), ("M", 3),
+    ("F", 6), ("E", 4), ("E", 1), ("M", 4), ("T", 5), ("F", 7), ("M", 2), ("E", 7, 0), ("T", 3),
+    ("E", 6), ("M", 7), ("T", 4), ("T", 7), ("M", 6), ("C", 3), ("M", 1), ("T", 2), ("T", 6),
+    ("M", 0), ("T", 1), ("C", 2), ("T", 0), ("C", 5), ("C", 1), ("C", 0), ("C", 4), ("C", 7),
+    ("C", 6),
+]
 
 
 def dot(left, right, axes=(1, 0)):
@@ -242,11 +251,11 @@
     return total
 
 
-def back(
+def experts_back(
     sp_count, tp_count, ready,
-    rows_ref, switch_ref, expand_ref, contract_ref, hidden_ref, slots, weight_ref, out_ref,
+    rows_ref, switch_ref, expand_ref, contract_ref, hidden_ref, slots, weights,
     y_ref, from_sib, pair, from_peer, summed, back,
-    s_sib, r_sib, s_peer, r_peer, s_back, r_back, s_own, s_fwd, r_col,
+    s_sib, r_sib, s_peer, r_peer, s_back, r_back, ending,
 ):
     sp, tp = lax.axis_index("sp"), lax.axis_index("tp")
     per, model = y_ref.shape[1:]
@@ -254,8 +263,13 @@
     cols = model // tp_count
     mine = span(tp, cols)
     groups = tp_count // 2
-    core, group = lax.rem(tp, 2), tp // 2
+    core, group = lax.rem(tp, 2), lax.div(tp, 2)
     sibling = group * 2 + 1 - core
+    others = [lax.rem(group + d, groups) for d in range(1, groups)]
+    local = switch_ref.shape[0]
+    capacity = per // local
+    top = len(slots)
+    places = lax.broadcasted_iota(jnp.int32, (rows, per), 1)
 
     def sib_copy(s, g):
         return copy_to(
@@ -278,16 +292,19 @@
     def back_copy(t):
         return copy_to(summed.at[t], back.at[sp], s_back.at[t], r_back.at[sp], {"sp": t})
 
-    def others():
-        return [lax.rem(group + d, groups) for d in range(1, groups)]
-
-    local = switch_ref.shape[0]
-    capacity = per // local
-    chunk = math.gcd(sp_count, max(1, 256 // capacity))
-    chunks = sp_count // chunk
-    half = sp_count // 2
-    ranks = list(range(half, sp_count)) + list(range(half - 1, -1, -1))
-    order = [mate(sp, d, sp_count) for d in ranks]
+    def close(s, carry):
+        sib_copy(s, group).wait_send()
+        for g in others:
+            sib_copy(s, g).wait_send()
+            peer_copy(s, g).wait_send()
+        return carry
+
+    def sent(d, carry):
+        back_copy(lax.rem(sp + d, sp_count)).wait_send()
+        return carry
+
+    ending.append(lambda: lax.fori_loop(0, sp_count, close, 0))
+    ending.append(lambda: lax.fori_loop(1, sp_count, sent, 0))
 
     def expert(at):
         for s in at:
@@ -298,15 +315,15 @@
             gate = dot(data, switch_ref[e])
             units = (gate / (1.0 + jnp.exp(-gate)) * dot(data, expand_ref[e])).astype(BF16)
             value = dot(units, contract_ref[e]).astype(BF16)
-            for c in range(chunk):
-                y_ref[at[c], inside, :] = value[c * capacity : (c + 1) * capacity]
+            for c, s in enumerate(at):
+                y_ref[s, inside, :] = value[c * capacity : (c + 1) * capacity]
         for s in at:
-            for g in others():
+            for g in others:
                 sib_copy(s, g).start()
             sib_copy(s, group).start()
 
     def meet(s):
-        for g in others():
+        for g in others:
             sib_copy(s, g).wait_recv()
             pair[s, g] = (
                 y_ref[s, :, span(g * 2 + core, cols)].astype(F32) + from_sib[s, g].astype(F32)
@@ -316,7 +333,7 @@
     def total_up(s, own):
         sib_copy(s, group).wait_recv()
         total = y_ref[s, :, mine].astype(F32) + from_sib[s, group].astype(F32)
-        for g in others():
+        for g in others:
             copy_to(
                 from_peer.at[s, g],
                 from_peer.at[s, g],
@@ -331,32 +348,31 @@
             summed[s] = total.astype(BF16)
             back_copy(s).start()
 
-    for i in range(chunks + 1):
-        if i < chunks:
-            at = order[i * chunk : (i + 1) * chunk]
-            expert(at)
-            for s in at:
-                meet(s)
-        if i:
-            for c in range((i - 1) * chunk, i * chunk):
-                total_up(order[c], ranks[c] == 0)
-    weights = weight_ref[...]
-    places = lax.broadcasted_iota(jnp.int32, (rows, per), 1)
-    top = len(slots)
-    result = hidden_ref[...]
-    landing = ranks[: half - 1] + ranks[half:] + [ranks[half - 1]]
-    for d in landing:
-        s = mate(sp, d, sp_count)
-        if d:
+    def combine(s, own):
+        if not own:
             copy_to(back.at[s], back.at[s], s_back.at[s], r_back.at[s], {"sp": s}).wait_recv()
         chosen = [
-            jnp.where(slots[k] == places + s * per, 1.0, 0.0).astype(BF16)
-            for k in range(top)
+            jnp.where(slots[k] == places + s * per, 1.0, 0.0).astype(BF16) for k in range(top)
         ]
         picked = dot(stack(*chosen), back[s])
+        total = hidden_ref[...]
         for k in range(top):
-            result = result + weights[:, k : k + 1] * picked[k * rows : (k + 1) * rows]
-    out_ref[:, mine] = result.astype(BF16)
+            total = total + weights[k] * picked[k * rows : (k + 1) * rows]
+        hidden_ref[...] = total
+
+    return expert, meet, total_up, combine
+
+
+def gather_out(tp_count, hidden_ref, out_ref, s_own, s_fwd, r_col):
+    tp = lax.axis_index("tp")
+    model = out_ref.shape[1]
+    cols = model // tp_count
+    mine = span(tp, cols)
+    groups = tp_count // 2
+    core, group = lax.rem(tp, 2), lax.div(tp, 2)
+    sibling = group * 2 + 1 - core
+    others = [lax.rem(group + d, groups) for d in range(1, groups)]
+    out_ref[:, mine] = hidden_ref[...].astype(BF16)
 
     def own_copy(p):
         here = out_ref.at[:, mine]
@@ -366,7 +382,7 @@
         here = out_ref.at[:, span(o, cols)]
         return copy_to(here, here, s_fwd.at[o], r_col.at[o], {"tp": sibling})
 
-    peers = [g * 2 + core for g in others()]
+    peers = [g * 2 + core for g in others]
     for p in peers:
         own_copy(p).start()
     own_copy(sibling).start()
@@ -374,35 +390,38 @@
         forward(p).wait_recv()
         forward(p).start()
     forward(sibling).wait_recv()
-    for g in others():
+    for g in others:
         forward(g * 2 + 1 - core).wait_recv()
     own_copy(sibling).wait_send()
     for p in peers:
         own_copy(p).wait_send()
         forward(p).wait_send()
 
-    def close(s, carry):
-        sib_copy(s, group).wait_send()
-        for g in others():
-            sib_copy(s, g).wait_send()
-            peer_copy(s, g).wait_send()
-        return carry
-
-    lax.fori_loop(0, sp_count, close, 0)
-
-    def sent(d, carry):
-        back_copy(lax.rem(sp + d, sp_count)).wait_send()
-        return carry
-
-    lax.fori_loop(1, sp_count, sent, 0)
+
+def plan(count, capacity):
+    half = count // 2
+    near, far = list(range(half)), list(range(half, count))
+    if count == 8 and capacity == 128:
+        return SENDS, SCRIPT
+    chunk = max(1, 256 // capacity)
+    steps = []
+    for d in near + far:
+        steps += [("R", d), ("F", d)]
+    ranks = far + near[::-1]
+    for i in range(0, count, chunk):
+        steps.append(("E", *ranks[i : i + chunk]))
+        steps += [("M", d) for d in ranks[i : i + chunk]]
+        steps += [("T", d) for d in ranks[i : i + chunk]]
+    return near[1:] + far, steps + [("C", d) for d in ranks]
 
 
 def layer_kernel(
     head_dim, segment, sp_count, tp_count, experts, capacity,
     q_in, k_in, v_in, a_in, f_in, b_in, w_in, skip_in, switch_in, expand_in, contract_in,
-    norm_ref, gain_ref, ids_ref, weight_ref,
+    norm_in, gain_in, ids_in, chance_in, within_in,
     out_ref,
-    q_ref, k_ref, v_ref, a_ref, f_ref, b_ref, w_ref, skip_ref, s_in,
+    q_ref, k_ref, v_ref, a_ref, f_ref, b_ref, w_ref, skip_ref,
+    norm_ref, gain_ref, ids_ref, chance_ref, within_ref, s_in,
     local, maps_in, ka, got, fold, st, mixed,
     lent, kept, from_sib, pair, from_peer, squares, outgoing,
     s_map, r_map, s_fold, r_fold, s_sib, r_sib, s_peer, r_peer,
@@ -426,15 +445,20 @@
         pltpu.make_async_copy(src, dst, s_in.at[i])
         for i, (src, dst) in enumerate(
             [(f_in, f_ref), (b_in, b_ref), (k_in, k_ref), (a_in, a_ref), (q_in, q_ref),
-             (v_in, v_ref), (w_in, w_ref), (skip_in, skip_ref), (switch_in, switch_ref),
-             (expand_in, expand_ref), (contract_in, contract_ref)]
+             (v_in, v_ref), (norm_in, norm_ref), (gain_in, gain_ref), (ids_in, ids_ref),
+             (chance_in, chance_ref), (within_in, within_ref), (w_in, w_ref),
+             (skip_in, skip_ref), (switch_in, switch_ref), (expand_in, expand_ref),
+             (contract_in, contract_ref)]
         )
     ]
-    for copy in early:
+    for copy in early[:6]:
         copy.start()
     call_peers(sp_count, tp_count, sp, tp)
     for copy in early[:6]:
         copy.wait()
+    for copy in early[6:]:
+        copy.start()
+    ending = []
 
     def unless_me(t, action):
         pl.when(t != sp)(action)
@@ -472,17 +496,35 @@
         head_dim, segment, q_ref, k_ref, v_ref, a_ref, f_ref, b_ref, emit_map, send_maps, emit_rows
     )
 
-    ids = ids_ref[...]
-    top = ids.shape[1]
-    lanes = lax.broadcasted_iota(jnp.int32, (rows, experts), 1)
-    named = [ids[:, k : k + 1] == lanes for k in range(top)]
+    for copy in early[6:]:
+        copy.wait()
+    top = ids_ref.shape[0]
+    within = within_ref[...]
+    shares = chance_ref[...] * within / jnp.sum(within, axis=0, keepdims=True)
+    lines = [ids_ref[k : k + 1, :].astype(F32) for k in range(top)]
+    lines = lines + [shares[k : k + 1, :] for k in range(top)]
+    place = lax.broadcasted_iota(jnp.int32, (8, rows), 0)
+    table = jnp.zeros((8, rows), F32)
+    for k in range(2 * top):
+        table = jnp.where(place == k, lines[k], table)
+    pieces = stack(*[piece.astype(F32) for piece in thirds(table)]).astype(BF16)
+    unit = jnp.where(
+        lax.rem(lax.broadcasted_iota(jnp.int32, (24, 128), 0), 8)
+        == lax.broadcasted_iota(jnp.int32, (24, 128), 1),
+        1.0,
+        0.0,
+    ).astype(BF16)
+    upright = dot(pieces, unit, (0, 0))
+    weights = [upright[:, top + k : top + k + 1] for k in range(top)]
+    lanes = lax.broadcasted_iota(jnp.int32, (rows, experts), 1).astype(F32)
+    named = [upright[:, k : k + 1] == lanes for k in range(top)]
     anyone = sum(jnp.where(n, 1.0, 0.0) for n in named).astype(BF16)
     r0 = lax.broadcasted_iota(jnp.int32, (rows, rows), 0)
     r1 = lax.broadcasted_iota(jnp.int32, (rows, rows), 1)
     before = dot(jnp.where(r0 > r1, 1.0, 0.0).astype(BF16), anyone)
     slots = [
         jnp.sum(
-            jnp.where(n, before + lanes.astype(F32) * capacity, 0.0), axis=1, keepdims=True
+            jnp.where(n, before + lanes * capacity, 0.0), axis=1, keepdims=True
         ).astype(jnp.int32)
         for n in named
     ]
@@ -507,6 +549,16 @@
                 state[i] = product[:head_dim] + product[head_dim:] + both[:, head_dim:].astype(F32)
         st[pl.ds(sp * share, share)] = fold[sp]
 
+    def map_sent():
+        for t in range(workers):
+            unless_me(t, lambda t=t: map_copy(t, sp).wait_send())
+
+    def fold_sent():
+        for t in range(sp_count):
+            unless_me(t, lambda t=t: fold_copy(t, sp).wait_send())
+
+    ending.append(map_sent)
+    ending.append(fold_sent if workers == sp_count else lambda: pl.when(sp < workers)(fold_sent))
     if workers == sp_count:
         chain()
     else:
@@ -541,8 +593,8 @@
             pair.at[g], from_peer.at[group], s_peer.at[g], r_peer.at[group], {"tp": g * 2 + core}
         )
 
-    for copy in early[6:8]:
-        copy.wait()
+    ending.append(lambda: [sib_copy(g).wait_send() for g in others + [group]])
+    ending.append(lambda: [peer_copy(g).wait_send() for g in others])
     for g in others + [group]:
         lent[g] = dot(mixed[...], w_ref[:, span(g * 2 + 1 - core, cols)]).astype(BF16)
         sib_copy(g).start()
@@ -565,6 +617,9 @@
     def square_copy(p):
         return copy_to(squares.at[tp], squares.at[tp], s_sq.at[p], r_sq.at[tp], {"tp": p})
 
+    ending.append(
+        lambda: [square_copy(lax.rem(tp + d, tp_count)).wait_send() for d in range(1, tp_count)]
+    )
     for d in range(1, tp_count):
         square_copy(lax.rem(tp + d, tp_count)).start()
     total = squares[tp]
@@ -612,48 +667,6 @@
             own_copy(p, s).start()
         own_copy(sibling, s).start()
 
-    near, far = list(range(1, sp_count // 2)), list(range(sp_count // 2, sp_count))
-    sending, landing = [], [0]
-    for i, d in enumerate(far):
-        sending += near[i : i + 1] + [d]
-    landing = [0] + near[:2] + sum([[d] + near[i + 2 : i + 3] for i, d in enumerate(far)], [])
-    for d in sending[:2]:
-        outgoing[mate(sp, d, sp_count)] = block_for(mate(sp, d, sp_count))
-        out_copy(mate(sp, d, sp_count)).start()
-    rows_ref[sp, :, mine] = block_for(sp)
-    pass_on(sp)
-    for d in sending[2:]:
-        outgoing[mate(sp, d, sp_count)] = block_for(mate(sp, d, sp_count))
-        out_copy(mate(sp, d, sp_count)).start()
-    lag = 2
-
-    def relay(i):
-        if i < sp_count:
-            s = mate(sp, landing[i], sp_count)
-            here = rows_ref.at[s, :, mine]
-            copy_to(here, here, s_out.at[s], r_out.at[s], {"sp": s}).wait_recv()
-            pass_on(s)
-        if i >= lag:
-            s = mate(sp, landing[i - lag], sp_count)
-            for o in peers:
-                forward(o, s).wait_recv()
-                forward(o, s).start()
-
-    def ready(s):
-        forward(sibling, s).wait_recv()
-        for g in others:
-            forward(g * 2 + 1 - core, s).wait_recv()
-
-    for i in range(1, sp_count + lag):
-        relay(i)
-    for copy in early[8:]:
-        copy.wait()
-    back(
-        sp_count, tp_count, ready,
-        rows_ref, switch_ref, expand_ref, contract_ref, hidden_ref, slots, weight_ref, out_ref,
-        *back_refs,
-    )
-
     def settle(s, carry):
         own_copy(sibling, s).wait_send()
         for p in peers:
@@ -661,30 +674,58 @@
             forward(p, s).wait_send()
         return carry
 
-    lax.fori_loop(0, sp_count, settle, 0)
-
     def sent(d, carry):
         out_copy(lax.rem(sp + d, sp_count)).wait_send()
         return carry
 
-    lax.fori_loop(1, sp_count, sent, 0)
-    for d in range(1, tp_count):
-        square_copy(lax.rem(tp + d, tp_count)).wait_send()
-    for g in others:
-        sib_copy(g).wait_send()
-        peer_copy(g).wait_send()
-    sib_copy(group).wait_send()
-    for t in range(workers):
-        unless_me(t, lambda t=t: map_copy(t, sp).wait_send())
-
-    def folded():
-        for t in range(sp_count):
-            unless_me(t, lambda t=t: fold_copy(t, sp).wait_send())
-
-    if workers == sp_count:
-        folded()
-    else:
-        pl.when(sp < workers)(folded)
+    ending.append(lambda: lax.fori_loop(0, sp_count, settle, 0))
+    ending.append(lambda: lax.fori_loop(1, sp_count, sent, 0))
+    def ready(s):
+        forward(sibling, s).wait_recv()
+        for g in others:
+            forward(g * 2 + 1 - core, s).wait_recv()
+
+    sends, steps = plan(sp_count, capacity)
+
+    def source(d):
+        return mate(sp, d, sp_count)
+
+    y_ref, sib_back, pair_back, peer_back, summed, returned = back_refs[:6]
+    s_sib2, r_sib2, s_peer2, r_peer2, s_back, r_back, s_last, s_fwd2, r_last = back_refs[6:]
+    for d in sends:
+        t = mate(sp, d, sp_count)
+        outgoing[t] = block_for(t)
+        out_copy(t).start()
+    rows_ref[sp, :, mine] = block_for(sp)
+    expert, meet, total_up, combine = experts_back(
+        sp_count, tp_count, ready,
+        rows_ref, switch_ref, expand_ref, contract_ref, hidden_ref, slots, weights,
+        y_ref, sib_back, pair_back, peer_back, summed, returned,
+        s_sib2, r_sib2, s_peer2, r_peer2, s_back, r_back, ending,
+    )
+    for kind, *which in steps:
+        for d in which[:1] if kind == "E" else which:
+            s = source(d)
+            if kind == "R":
+                if d:
+                    here = rows_ref.at[s, :, mine]
+                    copy_to(here, here, s_out.at[s], r_out.at[s], {"sp": s}).wait_recv()
+                pass_on(s)
+            if kind == "F":
+                for o in peers:
+                    forward(o, s).wait_recv()
+                    forward(o, s).start()
+            if kind == "E":
+                expert([source(i) for i in which])
+            if kind == "M":
+                meet(s)
+            if kind == "T":
+                total_up(s, d == 0)
+            if kind == "C":
+                combine(s, d == 0)
+    gather_out(tp_count, hidden_ref, out_ref, s_last, s_fwd2, r_last)
+    for wait in ending:
+        wait()
 
 
 def body(
@@ -721,17 +762,12 @@
     vmem = pl.BlockSpec(memory_space=pltpu.VMEM)
     hbm = pl.BlockSpec(memory_space=pltpu.HBM)
     sems = pltpu.SemaphoreType.DMA
-    route_weight = (
-        cluster_router_chance[:, None]
-        * specialist_chance_within_cluster
-        / jnp.sum(specialist_chance_within_cluster, axis=1, keepdims=True)
-    )
     return pl.pallas_call(
         functools.partial(
             layer_kernel, head_dim, min(64, tok_rows), sp_count, tp_count, experts, capacity
         ),
         out_shape=jax.ShapeDtypeStruct((tok_rows, model_width), BF16),
-        in_specs=[hbm] * 11 + [vmem] * 4,
+        in_specs=[hbm] * 16,
         out_specs=vmem,
         scratch_shapes=[
             pltpu.VMEM((tok_rows, channels), BF16),
@@ -742,7 +778,12 @@
             pltpu.VMEM((heads, tok_rows), F32),
             pltpu.VMEM((channels, model_width), BF16),
             pltpu.VMEM((tok_rows, model_width), BF16),
-            sems((11,)),
+            pltpu.VMEM((1, channels), F32),
+            pltpu.VMEM((1, model_width), F32),
+            pltpu.VMEM((top_count, tok_rows), jnp.int32),
+            pltpu.VMEM((1, tok_rows), F32),
+            pltpu.VMEM((top_count, tok_rows), F32),
+            sems((16,)),
             pltpu.VMEM((tok_rows, channels), F32),
             pltpu.VMEM((tok_rows, channels), BF16),
             pltpu.VMEM((heads, head_dim, 2 * head_dim), BF16),
@@ -810,8 +851,9 @@
         specialist_contraction_matrix,
         subspace_normalizer_gain.reshape(1, channels),
         specialist_prenormal_gain.reshape(1, model_width),
-        chosen_specialist_ids,
-        route_weight,
+        chosen_specialist_ids.T,
+        cluster_router_chance.reshape(1, tok_rows),
+        specialist_chance_within_cluster.T,
     )
 
 

time: 113 us -> 104 us (0.920)
  Pallas kernels: 107 us -> 101 us
  local copies, waits for them, and re-layouts: 3.91 us -> 2.3 us
  other arithmetic: 1.47 us -> 0 us
    pallas_call x1, Pallas kernels: 107 us -> 101 us  [body(): pl.pallas_call(functools.partial(layer_kernel, head_dim, min(64, tok_rows...]
    unnamed x2 -> x1, local copies, waits for them, and re-layouts: 3.78 us -> 2.3 us
where the time goes in v3:
time: 104 us; the launch traced here: 103 us
  Pallas kernels  101 us (97%)
  local copies, waits for them, and re-layouts  2.3 us (2%)
    pallas_call x1, Pallas kernels, body(): pl.pallas_call(functools.partial(layer_kernel, head_dim, min(64, tok_rows...  101 us
    unnamed x1, local copies, waits for them, and re-layouts  2.3 us

profile of v3, /device:TPU:0, one launch (start us, length us, event | category | flops | bytes accessed | tf_op | source)
XLA Modules:
  0.0 103.4 jit_solution(13713349121296441978)
XLA Ops:
  0.0 101.0 %shard_map.154 = bf16[256,2048]{1,0:T(8,128)(2,1)} custom-call(bf16[256,512]{1,0:T(8,128)(2,1)} %q_in.1, bf16[256,512]{1,0:T(8,128)(2,1)} %k_in.1, bf16[256,512]{1,0:T(8,128)(2,1)} %v_in.1, bf16[256,512]{1,0:T(8,128)(2,1)} %a_in.1, f32[256,512]{1,0:T(8,128)} %f_in.1, f32[8,256]{1,0:T(8,128)} %bitcast.6, bf16[512,2048]{1,0:T(8,128)(2,1)} %w_in.1, ...), custom_call_target="tpu_custom_call" | custom-call | tf_op jit(solution)/shard_map/pallas_call | solution.py:765
  101.1 2.3 %copy.18 = bf16[256,2048]{1,0:T(8,128)(2,1)} copy(bf16[256,2048]{1,0:T(8,128)(2,1)} %shard_map.154) | data formatting | bytes 2097152

commit v4 on v3

--- a/solution.py
+++ b/solution.py
@@ -11,7 +11,7 @@
 MESH = pl.DeviceIdType.MESH
 F32 = jnp.float32
 BF16 = jnp.bfloat16
-VMEM_LIMIT = 63 * 1024 * 1024
+VMEM_LIMIT = 48 * 1024 * 1024
 SENDS = [6, 1, 5, 2, 3, 4, 7]
 SCRIPT = [
     ("R", 1), ("R", 0), ("R", 6), ("R", 5), ("R", 2), ("R", 3), ("F", 5), ("F", 0), ("F", 2),
@@ -252,7 +252,7 @@
 
 
 def experts_back(
-    sp_count, tp_count, ready,
+    sp_count, tp_count, ready, scale_of,
     rows_ref, switch_ref, expand_ref, contract_ref, hidden_ref, slots, weights,
     y_ref, from_sib, pair, from_peer, summed, back,
     s_sib, r_sib, s_peer, r_peer, s_back, r_back, ending,
@@ -306,14 +306,17 @@
     ending.append(lambda: lax.fori_loop(0, sp_count, close, 0))
     ending.append(lambda: lax.fori_loop(1, sp_count, sent, 0))
 
-    def expert(at):
+    def expert(at, own):
         for s in at:
             ready(s)
+        scales = [scale_of(s, o) for s, o in zip(at, own)]
         for e in range(local):
             inside = slice(e * capacity, (e + 1) * capacity)
             data = jnp.concatenate([rows_ref[s, inside, :] for s in at], axis=0)
-            gate = dot(data, switch_ref[e])
-            units = (gate / (1.0 + jnp.exp(-gate)) * dot(data, expand_ref[e])).astype(BF16)
+            scale = jnp.concatenate([c[inside] for c in scales], axis=0)
+            gate = dot(data, switch_ref[e]) * scale
+            wide = dot(data, expand_ref[e]) * scale
+            units = (gate / (1.0 + jnp.exp(-gate)) * wide).astype(BF16)
             value = dot(units, contract_ref[e]).astype(BF16)
             for c, s in enumerate(at):
                 y_ref[s, inside, :] = value[c * capacity : (c + 1) * capacity]
@@ -426,7 +429,8 @@
     lent, kept, from_sib, pair, from_peer, squares, outgoing,
     s_map, r_map, s_fold, r_fold, s_sib, r_sib, s_peer, r_peer,
     s_sq, r_sq, s_out, r_out, s_own, s_fwd, r_col,
-    hidden_ref, rows_ref, switch_ref, expand_ref, contract_ref, *back_refs,
+    hidden_ref, rows_ref, switch_ref, expand_ref, contract_ref,
+    scale_out, scale_in, s_scale, r_scale, *back_refs,
 ):
     sp, tp = lax.axis_index("sp"), lax.axis_index("tp")
     rows, channels = q_in.shape
@@ -622,30 +626,20 @@
     )
     for d in range(1, tp_count):
         square_copy(lax.rem(tp + d, tp_count)).start()
-    total = squares[tp]
-    for d in range(1, tp_count):
-        p = lax.rem(tp + d, tp_count)
-        copy_to(squares.at[p], squares.at[p], s_sq.at[p], r_sq.at[p], {"tp": p}).wait_recv()
-        total = total + squares[p]
-    inverse = lax.rsqrt(total / model + 1e-06)
-    first = jnp.where(lax.broadcasted_iota(jnp.int32, (8, 128), 0) == 0, 1.0, 0.0).astype(BF16)
-    column = None
-    for _ in range(3):
-        piece = inverse.astype(BF16)
-        inverse = inverse - piece.astype(F32)
-        product = dot(piece, first, (0, 0))
-        column = product if column is None else column + product
-    normed = (hidden * column[:, :1] * gain_ref[:, mine]).astype(BF16)
+    normed = (hidden * gain_ref[:, mine]).astype(BF16)
 
     per = experts // sp_count * capacity
     places = lax.broadcasted_iota(jnp.int32, (rows, per), 1)
 
-    def block_for(t):
+    def chosen_for(t):
         at = places + t * per
         chosen = slots[0] == at
         for s in slots[1:]:
             chosen = chosen | (s == at)
-        return dot(jnp.where(chosen, 1.0, 0.0).astype(BF16), normed, (0, 0)).astype(BF16)
+        return jnp.where(chosen, 1.0, 0.0).astype(BF16)
+
+    def block_for(t):
+        return dot(chosen_for(t), normed, (0, 0)).astype(BF16)
 
     def out_copy(t):
         return copy_to(
@@ -697,8 +691,47 @@
         outgoing[t] = block_for(t)
         out_copy(t).start()
     rows_ref[sp, :, mine] = block_for(sp)
+    total = squares[tp]
+    for d in range(1, tp_count):
+        p = lax.rem(tp + d, tp_count)
+        copy_to(squares.at[p], squares.at[p], s_sq.at[p], r_sq.at[p], {"tp": p}).wait_recv()
+        total = total + squares[p]
+    inverse = [piece.astype(F32) for piece in thirds(lax.rsqrt(total / model + 1e-06))]
+    inverse = stack(*inverse).astype(BF16)
+
+    def scale_for(t):
+        product = dot(inverse, chosen_for(t))
+        return product[:8] + product[8:16] + product[16:]
+
+    def scale_copy(t):
+        return copy_to(
+            scale_out.at[t], scale_in.at[sp], s_scale.at[t], r_scale.at[sp], {"sp": t}
+        )
+
+    def scale_sent(d, carry):
+        scale_copy(lax.rem(sp + d, sp_count)).wait_send()
+        return carry
+
+    ending.append(lambda: lax.fori_loop(1, sp_count, scale_sent, 0))
+    for d in sends:
+        t = mate(sp, d, sp_count)
+        scale_out[t] = scale_for(t)
+        scale_copy(t).start()
+    scale_in[sp] = scale_for(sp)
+    one = jnp.where(
+        lax.rem(lax.broadcasted_iota(jnp.int32, (24, 128), 0), 8) == 0, 1.0, 0.0
+    ).astype(BF16)
+
+    def scale_of(s, own):
+        if not own:
+            copy_to(
+                scale_in.at[s], scale_in.at[s], s_scale.at[s], r_scale.at[s], {"sp": s}
+            ).wait_recv()
+        pieces = stack(*[piece.astype(F32) for piece in thirds(scale_in[s])]).astype(BF16)
+        return dot(pieces, one, (0, 0))[:, :1]
+
     expert, meet, total_up, combine = experts_back(
-        sp_count, tp_count, ready,
+        sp_count, tp_count, ready, scale_of,
         rows_ref, switch_ref, expand_ref, contract_ref, hidden_ref, slots, weights,
         y_ref, sib_back, pair_back, peer_back, summed, returned,
         s_sib2, r_sib2, s_peer2, r_peer2, s_back, r_back, ending,
@@ -716,7 +749,7 @@
                     forward(o, s).wait_recv()
                     forward(o, s).start()
             if kind == "E":
-                expert([source(i) for i in which])
+                expert([source(i) for i in which], [i == 0 for i in which])
             if kind == "M":
                 meet(s)
             if kind == "T":
@@ -818,6 +851,10 @@
             pltpu.VMEM(specialist_switch_matrix.shape, BF16),
             pltpu.VMEM(specialist_expansion_matrix.shape, BF16),
             pltpu.VMEM(specialist_contraction_matrix.shape, BF16),
+            pltpu.VMEM((sp_count, 8, per), F32),
+            pltpu.VMEM((sp_count, 8, per), F32),
+            sems((sp_count,)),
+            sems((sp_count,)),
             pltpu.VMEM((sp_count, per, model_width), BF16),
             pltpu.VMEM((sp_count, groups, per, cols), BF16),
             pltpu.VMEM((sp_count, groups, per, cols), BF16),
@@ -838,22 +875,27 @@
             collective_id=1, has_side_effects=True, vmem_limit_bytes=VMEM_LIMIT
         ),
     )(
-        readout_query_vectors,
-        attention_key_vectors,
-        attention_content_vectors,
-        step_size_preactivation,
-        forgetting_preactivation,
-        extra_forgetting_bias.T,
-        blender_projection_matrix,
-        skip_connection_stream,
-        specialist_switch_matrix,
-        specialist_expansion_matrix,
-        specialist_contraction_matrix,
-        subspace_normalizer_gain.reshape(1, channels),
-        specialist_prenormal_gain.reshape(1, model_width),
-        chosen_specialist_ids.T,
-        cluster_router_chance.reshape(1, tok_rows),
-        specialist_chance_within_cluster.T,
+        *[
+            pltpu.with_memory_space_constraint(operand, pltpu.HBM)
+            for operand in (
+                readout_query_vectors,
+                attention_key_vectors,
+                attention_content_vectors,
+                step_size_preactivation,
+                forgetting_preactivation,
+                extra_forgetting_bias.T,
+                blender_projection_matrix,
+                skip_connection_stream,
+                specialist_switch_matrix,
+                specialist_expansion_matrix,
+                specialist_contraction_matrix,
+                subspace_normalizer_gain.reshape(1, channels),
+                specialist_prenormal_gain.reshape(1, model_width),
+                chosen_specialist_ids.T,
+                cluster_router_chance.reshape(1, tok_rows),
+                specialist_chance_within_cluster.T,
+            )
+        ]
     )
 
 

time: 104 us -> 102 us (0.981)
  local copies, waits for them, and re-layouts: 2.3 us -> 0.97 us
    unnamed x1, local copies, waits for them, and re-layouts: 2.3 us -> 0.97 us
where the time goes in v4:
time: 102 us
  Pallas kernels  101 us (99%)
    pallas_call x1, Pallas kernels, body(): pl.pallas_call(functools.partial(layer_kernel, head_dim, min(64, tok_rows...  101 us

profile of v4, /device:TPU:0, one launch (start us, length us, event | category | flops | bytes accessed | tf_op | source)
XLA Modules:
  0.0 101.9 jit_solution(6909621393821765483)
XLA Ops:
  0.0 100.9 %shard_map.154 = bf16[256,2048]{1,0:T(8,128)(2,1)S(1)} custom-call(bf16[256,512]{1,0:T(8,128)(2,1)} %q_in.1, bf16[256,512]{1,0:T(8,128)(2,1)} %k_in.1, bf16[256,512]{1,0:T(8,128)(2,1)} %v_in.1, bf16[256,512]{1,0:T(8,128)(2,1)} %a_in.1, f32[256,512]{1,0:T(8,128)} %f_in.1, f32[8,256]{1,0:T(8,128)} %bitcast.6, bf16[512,2048]{1,0:T(8,128)(2,1)} %w_in.1, ...), custom_call_target="tpu_custom_call" | custom-call | tf_op jit(solution)/shard_map/pallas_call | solution.py:798
  100.9 1.0 copy.18

commit v5 on v4

--- a/solution.py
+++ b/solution.py
@@ -225,6 +225,11 @@
     pl.semaphore_wait(pltpu.get_barrier_semaphore(), sp_count + tp_count - 2)
 
 
+def cuts_of(rows):
+    size = rows // 2 if rows >= 128 else rows
+    return [(h, slice(h * size, (h + 1) * size)) for h in range(rows // size)]
+
+
 def copy_to(src, dst, send, recv, device):
     return pltpu.make_async_remote_copy(
         src_ref=src,
@@ -280,27 +285,33 @@
             {"tp": sibling},
         )
 
-    def peer_copy(s, g):
+    cuts = cuts_of(per)
+
+    def peer_copy(s, g, h, at):
         return copy_to(
-            pair.at[s, g],
-            from_peer.at[s, group],
-            s_peer.at[s, g],
-            r_peer.at[s, group],
+            pair.at[s, g, at],
+            from_peer.at[s, group, at],
+            s_peer.at[s, g, h],
+            r_peer.at[s, group, h],
             {"tp": g * 2 + core},
         )
 
-    def back_copy(t):
-        return copy_to(summed.at[t], back.at[sp], s_back.at[t], r_back.at[sp], {"sp": t})
+    def back_copy(t, h, at):
+        return copy_to(
+            summed.at[t, at], back.at[sp, at], s_back.at[t, h], r_back.at[sp, h], {"sp": t}
+        )
 
     def close(s, carry):
         sib_copy(s, group).wait_send()
         for g in others:
             sib_copy(s, g).wait_send()
-            peer_copy(s, g).wait_send()
+            for cut in cuts:
+                peer_copy(s, g, *cut).wait_send()
         return carry
 
     def sent(d, carry):
-        back_copy(lax.rem(sp + d, sp_count)).wait_send()
+        for cut in cuts:
+            back_copy(lax.rem(sp + d, sp_count), *cut).wait_send()
         return carry
 
     ending.append(lambda: lax.fori_loop(0, sp_count, close, 0))
@@ -328,32 +339,37 @@
     def meet(s):
         for g in others:
             sib_copy(s, g).wait_recv()
-            pair[s, g] = (
-                y_ref[s, :, span(g * 2 + core, cols)].astype(F32) + from_sib[s, g].astype(F32)
-            ).astype(BF16)
-            peer_copy(s, g).start()
+            for h, at in cuts:
+                pair[s, g, at] = (
+                    y_ref[s, at, span(g * 2 + core, cols)].astype(F32)
+                    + from_sib[s, g, at].astype(F32)
+                ).astype(BF16)
+                peer_copy(s, g, h, at).start()
 
     def total_up(s, own):
         sib_copy(s, group).wait_recv()
-        total = y_ref[s, :, mine].astype(F32) + from_sib[s, group].astype(F32)
-        for g in others:
-            copy_to(
-                from_peer.at[s, g],
-                from_peer.at[s, g],
-                s_peer.at[s, g],
-                r_peer.at[s, g],
-                {"tp": g * 2 + core},
-            ).wait_recv()
-            total = total + from_peer[s, g].astype(F32)
-        if own:
-            back[s] = total.astype(BF16)
-        else:
-            summed[s] = total.astype(BF16)
-            back_copy(s).start()
+        for h, at in cuts:
+            total = y_ref[s, at, mine].astype(F32) + from_sib[s, group, at].astype(F32)
+            for g in others:
+                copy_to(
+                    from_peer.at[s, g, at],
+                    from_peer.at[s, g, at],
+                    s_peer.at[s, g, h],
+                    r_peer.at[s, g, h],
+                    {"tp": g * 2 + core},
+                ).wait_recv()
+                total = total + from_peer[s, g, at].astype(F32)
+            if own:
+                back[s, at] = total.astype(BF16)
+            else:
+                summed[s, at] = total.astype(BF16)
+                back_copy(s, h, at).start()
 
     def combine(s, own):
         if not own:
-            copy_to(back.at[s], back.at[s], s_back.at[s], r_back.at[s], {"sp": s}).wait_recv()
+            for h, at in cuts:
+                here = back.at[s, at]
+                copy_to(here, here, s_back.at[s, h], r_back.at[s, h], {"sp": s}).wait_recv()
         chosen = [
             jnp.where(slots[k] == places + s * per, 1.0, 0.0).astype(BF16) for k in range(top)
         ]
@@ -641,43 +657,52 @@
     def block_for(t):
         return dot(chosen_for(t), normed, (0, 0)).astype(BF16)
 
-    def out_copy(t):
+    cuts = cuts_of(per)
+
+    def out_copy(t, h, at):
         return copy_to(
-            outgoing.at[t], rows_ref.at[sp, :, mine], s_out.at[t], r_out.at[sp], {"sp": t}
-        )
-
-    def own_copy(p, s):
-        here = rows_ref.at[s, :, mine]
-        return copy_to(here, here, s_own.at[p, s], r_col.at[tp, s], {"tp": p})
-
-    def forward(o, s):
-        here = rows_ref.at[s, :, span(o, cols)]
-        return copy_to(here, here, s_fwd.at[o, s], r_col.at[o, s], {"tp": sibling})
+            outgoing.at[t, at], rows_ref.at[sp, at, mine], s_out.at[t, h], r_out.at[sp, h], {"sp": t}
+        )
+
+    def own_copy(p, s, h, at):
+        here = rows_ref.at[s, at, mine]
+        return copy_to(here, here, s_own.at[p, s, h], r_col.at[tp, s, h], {"tp": p})
+
+    def forward(o, s, h, at):
+        here = rows_ref.at[s, at, span(o, cols)]
+        return copy_to(here, here, s_fwd.at[o, s, h], r_col.at[o, s, h], {"tp": sibling})
 
     peers = [g * 2 + core for g in others]
 
-    def pass_on(s):
-        for p in peers:
-            own_copy(p, s).start()
-        own_copy(sibling, s).start()
+    def pass_on(s, arrival=None):
+        for cut in cuts:
+            if arrival is not None:
+                arrival(*cut).wait_recv()
+            for p in peers:
+                own_copy(p, s, *cut).start()
+            own_copy(sibling, s, *cut).start()
 
     def settle(s, carry):
-        own_copy(sibling, s).wait_send()
-        for p in peers:
-            own_copy(p, s).wait_send()
-            forward(p, s).wait_send()
+        for cut in cuts:
+            own_copy(sibling, s, *cut).wait_send()
+            for p in peers:
+                own_copy(p, s, *cut).wait_send()
+                forward(p, s, *cut).wait_send()
         return carry
 
     def sent(d, carry):
-        out_copy(lax.rem(sp + d, sp_count)).wait_send()
+        for cut in cuts:
+            out_copy(lax.rem(sp + d, sp_count), *cut).wait_send()
         return carry
 
     ending.append(lambda: lax.fori_loop(0, sp_count, settle, 0))
     ending.append(lambda: lax.fori_loop(1, sp_count, sent, 0))
+
     def ready(s):
-        forward(sibling, s).wait_recv()
-        for g in others:
-            forward(g * 2 + 1 - core, s).wait_recv()
+        for cut in cuts:
+            forward(sibling, s, *cut).wait_recv()
+            for g in others:
+                forward(g * 2 + 1 - core, s, *cut).wait_recv()
 
     sends, steps = plan(sp_count, capacity)
 
@@ -689,7 +714,8 @@
     for d in sends:
         t = mate(sp, d, sp_count)
         outgoing[t] = block_for(t)
-        out_copy(t).start()
+        for cut in cuts:
+            out_copy(t, *cut).start()
     rows_ref[sp, :, mine] = block_for(sp)
     total = squares[tp]
     for d in range(1, tp_count):
@@ -739,15 +765,20 @@
     for kind, *which in steps:
         for d in which[:1] if kind == "E" else which:
             s = source(d)
-            if kind == "R":
-                if d:
-                    here = rows_ref.at[s, :, mine]
-                    copy_to(here, here, s_out.at[s], r_out.at[s], {"sp": s}).wait_recv()
+            if kind == "R" and d:
+
+                def arrival(h, at, s=s):
+                    here = rows_ref.at[s, at, mine]
+                    return copy_to(here, here, s_out.at[s, h], r_out.at[s, h], {"sp": s})
+
+                pass_on(s, arrival)
+            if kind == "R" and not d:
                 pass_on(s)
             if kind == "F":
-                for o in peers:
-                    forward(o, s).wait_recv()
-                    forward(o, s).start()
+                for cut in cuts:
+                    for o in peers:
+                        forward(o, s, *cut).wait_recv()
+                        forward(o, s, *cut).start()
             if kind == "E":
                 expert([source(i) for i in which], [i == 0 for i in which])
             if kind == "M":
@@ -788,6 +819,7 @@
     cols = model_width // tp_count
     per = local_experts * capacity
     groups = tp_count // 2
+    pieces = len(cuts_of(per))
     channels = readout_query_vectors.shape[1]
     heads = extra_forgetting_bias.shape[1]
     head_dim = channels // heads
@@ -841,11 +873,11 @@
             sems((groups,)),
             sems((tp_count,)),
             sems((tp_count,)),
-            sems((sp_count,)),
-            sems((sp_count,)),
-            sems((tp_count, sp_count)),
-            sems((tp_count, sp_count)),
-            sems((tp_count, sp_count)),
+            sems((sp_count, pieces)),
+            sems((sp_count, pieces)),
+            sems((tp_count, sp_count, pieces)),
+            sems((tp_count, sp_count, pieces)),
+            sems((tp_count, sp_count, pieces)),
             pltpu.VMEM((tok_rows, cols), F32),
             pltpu.VMEM((sp_count, per, model_width), BF16),
             pltpu.VMEM(specialist_switch_matrix.shape, BF16),
@@ -863,10 +895,10 @@
             pltpu.VMEM((sp_count, per, cols), BF16),
             sems((sp_count, groups)),
             sems((sp_count, groups)),
-            sems((sp_count, groups)),
-            sems((sp_count, groups)),
-            sems((sp_count,)),
-            sems((sp_count,)),
+            sems((sp_count, groups, pieces)),
+            sems((sp_count, groups, pieces)),
+            sems((sp_count, pieces)),
+            sems((sp_count, pieces)),
             sems((tp_count,)),
             sems((tp_count,)),
             sems((tp_count,)),

time: 102 us -> 103 us (level)
    pallas_call x1, Pallas kernels: 101 us -> 102 us  [body(): pl.pallas_call(functools.partial(layer_kernel, head_dim, min(64, tok_rows...]
where the time goes in v5:
time: 103 us
  Pallas kernels  102 us (99%)
    pallas_call x1, Pallas kernels, body(): pl.pallas_call(functools.partial(layer_kernel, head_dim, min(64, tok_rows...  102 us

profile of v5, /device:TPU:0, one launch (start us, length us, event | category | flops | bytes accessed | tf_op | source)
XLA Modules:
  0.0 103.3 jit_solution(15466573207996999393)
XLA Ops:
  0.0 102.3 %shard_map.154 = bf16[256,2048]{1,0:T(8,128)(2,1)S(1)} custom-call(bf16[256,512]{1,0:T(8,128)(2,1)} %q_in.1, bf16[256,512]{1,0:T(8,128)(2,1)} %k_in.1, bf16[256,512]{1,0:T(8,128)(2,1)} %v_in.1, bf16[256,512]{1,0:T(8,128)(2,1)} %a_in.1, f32[256,512]{1,0:T(8,128)} %f_in.1, f32[8,256]{1,0:T(8,128)} %bitcast.6, bf16[512,2048]{1,0:T(8,128)(2,1)} %w_in.1, ...), custom_call_target="tpu_custom_call" | custom-call | tf_op jit(solution)/shard_map/pallas_call | solution.py:830
  102.3 1.0 copy.18
